TPU v7x, 32 devices: a whole 2x2x4 slice. The times are simulated.
32 devices in a mesh: fs: 4 (over z), rep: 4 (over y, x), tp: 2 (over core).
Axes of the slice: x: 2, y: 2, z: 4, core: 2. Of those that a mesh axis runs over, the one named last changes fastest.
Arguments:
- saved_inputs: bfloat16 [12288, 2048], P(('fs', 'rep')), may hold values from -6 to 6
- query_cotangent: bfloat16 [12288, 1024], P(('fs', 'rep'), 'tp'), may hold values from -0.053955078 to 0.053955078
- value_cotangent: bfloat16 [12288, 2048], P(('fs', 'rep'), 'tp'), may hold values from -0.053955078 to 0.053955078
- query_weight: float32 [2048, 1024], P('fs', 'tp'), may hold values from -0.125 to 0.125
- value_weight: float32 [2048, 2048], P('fs', 'tp'), may hold values from -0.125 to 0.125
- query_factor: bfloat16 [2048, 256], P('fs'), as said below
- value_factor: bfloat16 [2048, 256], P('fs'), as said below
- query_first: float32 [256, 1024], P('rep', 'tp'), may hold values from -6 to 6
- query_second: float32 [256, 1024], P('rep', 'tp'), may hold values from 0.3 to 3
- value_first: float32 [256, 2048], P('rep', 'tp'), may hold values from -6 to 6
- value_second: float32 [256, 2048], P('rep', 'tp'), may hold values from 0.3 to 3
Outputs:
- query_direction: float32 [2048, 1024], P('fs', 'tp')
- value_direction: float32 [2048, 2048], P('fs', 'tp')
- query_master: float32 [2048, 1024], P('fs', 'tp')
- value_master: float32 [2048, 2048], P('fs', 'tp')
- query_first_new: float32 [256, 1024], P('rep', 'tp')
- query_second_new: float32 [256, 1024], P('rep', 'tp')
- value_first_new: float32 [256, 2048], P('rep', 'tp')
- value_second_new: float32 [256, 2048], P('rep', 'tp')
- query_copy: bfloat16 [2048, 1024], P(None, 'tp')
- value_copy: bfloat16 [2048, 2048], P(None, 'tp')
Inputs may be any that keep to these rules, and one draw needn't show every extreme that they name: `query_factor`: A matrix of full rank. `value_factor`: A matrix of full rank.
All inputs are finite; a program needn't handle non-finite values.
Results may differ from a plain program's by a relative error of at most 0.012.
Values may be sent and summed in bfloat16 or wider, within the bound.
A program may use at most 128 MiB of HBM per device.

v0:
```python
import functools

import jax
import jax.numpy as jnp
from jax import lax
from jax.experimental import pallas as pl
from jax.experimental.pallas import tpu as pltpu
from jax.sharding import PartitionSpec as P

BETA_ONE = 0.8
BETA_TWO = 0.9
EPS_RATIO = 1e-08
EPS_NORM = 1e-06
RATE = 0.02
BF = jnp.bfloat16
F32 = jnp.float32


def moments(projected, first, second):
    first_new = BETA_ONE * first + (1.0 - BETA_ONE) * projected
    second_new = BETA_TWO * second + (1.0 - BETA_TWO) * projected * projected
    ratio = first_new / (jnp.sqrt(second_new) + EPS_RATIO)
    return (first_new, second_new, ratio)


def exchange(
    nz,
    nr,
    x_hbm,
    cq_hbm,
    cv_hbm,
    wq_hbm,
    wv_hbm,
    qf_hbm,
    vf_hbm,
    q1_hbm,
    q2_hbm,
    v1_hbm,
    v2_hbm,
    w_out,
    f_ref,
    ratio_ref,
    proj_out,
    scale_out,
    x_ref,
    cq_ref,
    cv_ref,
    wf_ref,
    wb_ref,
    low_ref,
    part_ref,
    rs_ref,
    z_ref,
    zg_ref,
    zh_ref,
    m1_ref,
    m2_ref,
    sq_ref,
    local_sem,
    f1_s,
    f1_r,
    w1_s,
    w1_r,
    f2_s,
    f2_r,
    w2_s,
    w2_r,
    rs_s,
    rs_r,
    zs_s,
    zs_r,
    zg_s,
    zg_r,
    ag_s,
    ag_r,
    tp_s,
    tp_r,
):
    z = lax.axis_index("fs")
    r = lax.axis_index("rep")
    t = lax.axis_index("tp")
    rows = qf_hbm.shape[0]
    part = rows // nr
    qc = cq_ref.shape[1]
    cols = w_out.shape[1]
    half = cols // 2
    width = w_out.shape[0]
    rank = low_ref.shape[2]
    own = rank // nr
    tokens = x_ref.shape[0]
    z_of = [lax.rem(z + k, nz) for k in range(nz)]
    z_from = [lax.rem(z + nz - k, nz) for k in range(nz)]
    r_of = [lax.rem(r + j, nr) for j in range(nr)]
    side = r + 1 - 2 * lax.rem(r, 2)
    over = lax.rem(r + 2, nr)
    corner = nr - 1 - r
    other = 1 - t

    def remote(src, dst, ss, rs, dev):
        return pltpu.make_async_remote_copy(
            src_ref=src,
            dst_ref=dst,
            send_sem=ss,
            recv_sem=rs,
            device_id=dev,
            device_id_type=pl.DeviceIdType.MESH,
        )

    def slab(zz, rr):
        return pl.ds(pl.multiple_of(zz * rows + rr * part, part), part)

    def fac_copy(src):
        return pltpu.make_async_copy(
            src,
            f_ref.at[t, pl.ds(pl.multiple_of(z * rows, rows), rows)],
            local_sem.at[0],
        )

    @pl.when(t == 0)
    def _():
        fac_copy(qf_hbm).start()

    @pl.when(t == 1)
    def _():
        fac_copy(vf_hbm).start()

    wq_in = pltpu.make_async_copy(wq_hbm, wf_ref.at[:, pl.ds(0, qc)], local_sem.at[1])
    wv_in = pltpu.make_async_copy(wv_hbm, wf_ref.at[:, pl.ds(qc, cols - qc)], local_sem.at[2])
    x_in = pltpu.make_async_copy(x_hbm, x_ref, local_sem.at[3])
    cq_in = pltpu.make_async_copy(cq_hbm, cq_ref, local_sem.at[4])
    cv_in = pltpu.make_async_copy(cv_hbm, cv_ref, local_sem.at[5])
    left, right = pl.ds(0, qc), pl.ds(qc, cols - qc)
    mom = [
        pltpu.make_async_copy(src, dst.at[:, at], local_sem.at[7 + n])
        for n, (src, dst, at) in enumerate(
            (
                (q1_hbm, m1_ref, left),
                (v1_hbm, m1_ref, right),
                (q2_hbm, m2_ref, left),
                (v2_hbm, m2_ref, right),
            )
        )
    ]
    for c in [wq_in, wv_in, x_in, cq_in, cv_in] + mom:
        c.start()

    barrier = pltpu.get_barrier_semaphore()
    peers = [(z_of[k], r, t) for k in range(1, nz)]
    peers += [(z, r_of[j], t) for j in range(1, nr)]
    peers += [(z, r, other)]
    for dev in peers:
        pl.semaphore_signal(
            barrier, inc=1, device_id=dev, device_id_type=pl.DeviceIdType.MESH
        )
    pl.semaphore_wait(barrier, len(peers))

    fac_copy(qf_hbm).wait()
    sends = []
    f1 = []
    for k in range(1, nz):
        here = f_ref.at[t, slab(z, r)]
        c = remote(here, here, f1_s.at[k - 1], f1_r.at[k - 1], (z_of[k], r, t))
        c.start()
        f1.append(c)
    wq_in.wait()
    wv_in.wait()
    wb_ref[...] = wf_ref[...].astype(BF)
    order = sorted(range(1, nz), key=lambda k: min(k, nz - k))
    w1 = {}
    for k in order:
        c = remote(
            wb_ref.at[pl.ds(pl.multiple_of(r * part, part), part)],
            w_out.at[slab(z, r)],
            w1_s.at[k - 1],
            w1_r.at[k - 1],
            (z_of[k], r, t),
        )
        c.start()
        w1[k] = c
    w_own = pltpu.make_async_copy(
        wb_ref, w_out.at[pl.ds(pl.multiple_of(z * rows, rows), rows)], local_sem.at[6]
    )
    w_own.start()

    f2 = []
    for k in range(1, nz):
        f1[k - 1].wait_recv()
        there = f_ref.at[t, slab(z_from[k], r)]
        for j in range(1, nr):
            n = (k - 1) * (nr - 1) + j - 1
            c = remote(there, there, f2_s.at[n], f2_r.at[n], (z, r_of[j], t))
            c.start()
            f2.append(c)
    for c in f2:
        c.wait_recv()
    w2 = {}

    def spread(k):
        w1[k].wait_recv()
        there = w_out.at[slab(z_from[k], r)]
        for n, dev in ((0, side), (1, over)):
            c = remote(there, there, w2_s.at[k - 1, n], w2_r.at[k - 1, n], (z, dev, t))
            c.start()
            w2[k, n] = c

    def relay(k):
        for n, src, dev, at in ((0, side, over, 0), (1, over, side, half)):
            w2[k, n].wait_recv()
            there = w_out.at[slab(z_from[k], src), pl.ds(at, half)]
            c = remote(
                there, there, w2_s.at[k - 1, 2 + n], w2_r.at[k - 1, 2 + n], (z, dev, t)
            )
            c.start()
            w2[k, 2 + n] = c

    stages = [[], [], []]
    for n, k in enumerate(order):
        stages[min(n, 2)].append(k)
    x_in.wait()
    tile = tokens // 3

    @pl.loop(0, 3)
    def _(i):
        span = pl.ds(pl.multiple_of(i * tile, tile), tile)
        low_ref[t, span] = jnp.dot(
            x_ref[span, :], f_ref[t], preferred_element_type=F32
        ).astype(BF)

    lx = remote(low_ref.at[t], low_ref.at[t], tp_s.at[1], tp_r.at[1], (z, r, other))
    lx.start()
    fx = remote(f_ref.at[t], f_ref.at[t], tp_s.at[0], tp_r.at[0], (z, r, other))
    fx.start()
    for k in stages[0]:
        spread(k)
    cq_in.wait()
    cv_in.wait()
    lx.wait_recv()
    dims = (((0,), (0,)), ((), ()))
    part_ref[:, :qc] = lax.dot_general(
        low_ref[0], cq_ref[...], dims, preferred_element_type=F32
    ).astype(BF)
    part_ref[:, qc:] = lax.dot_general(
        low_ref[1], cv_ref[...], dims, preferred_element_type=F32
    ).astype(BF)

    def low_rows(rr):
        return pl.ds(pl.multiple_of(rr * own, own), own)

    rsc = []
    for j in range(1, nr):
        c = remote(
            part_ref.at[low_rows(r_of[j])],
            rs_ref.at[j - 1],
            rs_s.at[j - 1],
            rs_r.at[j - 1],
            (z, r_of[j], t),
        )
        c.start()
        rsc.append(c)

    for k in stages[0]:
        relay(k)
    for c in rsc:
        c.wait_recv()
    total = part_ref[low_rows(r), :].astype(F32)
    for j in range(1, nr):
        total = total + rs_ref[j - 1].astype(F32)
    share = own // nz
    scatter = share % 16 == 0
    zc = []
    if scatter:
        zg_ref[...] = total.astype(BF)
    else:
        z_ref[z] = total.astype(BF)

    def z_rows(zz):
        return pl.ds(pl.multiple_of(zz * share, share), share)

    for k in range(1, nz):
        src = zg_ref.at[z_rows(z_of[k])] if scatter else z_ref.at[z]
        c = remote(src, z_ref.at[z], zs_s.at[k - 1], zs_r.at[k - 1], (z_of[k], r, t))
        c.start()
        zc.append(c)
    if scatter:
        z_ref[z] = zg_ref[z_rows(z), :]
    for k in stages[1]:
        spread(k)
    for c in zc:
        c.wait_recv()
    proj = z_ref[0].astype(F32)
    for k in range(1, nz):
        proj = proj + z_ref[k].astype(F32)
    gc = []
    if scatter:
        for c in zc:
            c.wait_send()
        zh = zh_ref
        zh[z_rows(z), :] = proj.astype(BF)
        for k in range(1, nz):
            here = zh.at[z_rows(z)]
            c = remote(here, here, zg_s.at[k - 1], zg_r.at[k - 1], (z_of[k], r, t))
            c.start()
            gc.append(c)
    for k in stages[1]:
        relay(k)
    for k in stages[2]:
        spread(k)
    for c in mom:
        c.wait()
    if scatter:
        for c in gc:
            c.wait_recv()
        proj = zh[...].astype(F32)
    proj_out[...] = proj
    _, _, ratio = moments(proj, m1_ref[...], m2_ref[...])
    ratio_ref[low_rows(r), :] = ratio.astype(BF)
    agc = []
    for j in range(1, nr):
        here = ratio_ref.at[low_rows(r)]
        c = remote(here, here, ag_s.at[j - 1], ag_r.at[j - 1], (z, r_of[j], t))
        c.start()
        agc.append(c)
    for k in stages[2]:
        relay(k)
    fx.wait_recv()
    for c in agc:
        c.wait_recv()
    step = min(256, width)

    def squares(i, acc):
        span = pl.ds(pl.multiple_of(i * step, step), step)
        a = jnp.dot(f_ref[0, span], ratio_ref[:, :qc], preferred_element_type=F32)
        b = jnp.dot(f_ref[1, span], ratio_ref[:, qc:], preferred_element_type=F32)
        a = jnp.sum(a * a, axis=0, keepdims=True)
        b = jnp.sum(b * b, axis=0, keepdims=True)
        return (acc[0] + a, acc[1] + b)

    qs, vs = lax.fori_loop(
        0,
        width // step,
        squares,
        (jnp.zeros((1, qc), F32), jnp.zeros((1, cols - qc), F32)),
    )
    qs = jnp.sum(qs, axis=1, keepdims=True)
    vs = jnp.sum(vs, axis=1, keepdims=True)
    row = lax.broadcasted_iota(jnp.int32, sq_ref.shape[1:], 0)
    sq_ref[t] = jnp.where(row == 0, qs / (width * qc * 2), vs / (width * (cols - qc) * 2))
    sx = remote(sq_ref.at[t], sq_ref.at[t], tp_s.at[2], tp_r.at[2], (z, r, other))
    sx.start()
    sx.wait_recv()
    scale_out[...] = lax.rsqrt(sq_ref[0] + sq_ref[1] + EPS_NORM)
    for k in range(1, nz):
        w2[k, 2].wait_recv()
        w2[k, 3].wait_recv()
    for c in f1 + list(w1.values()) + f2 + rsc + ([] if scatter else zc) + gc + agc + [fx, lx, sx] + list(w2.values()):
        c.wait_send()
    w_own.wait()


def run_exchange(nz, nr, x, cq, cv, wq, wv, qf, vf, q1, q2, v1, v2):
    tokens, width = x.shape
    qc = cq.shape[1]
    cols = qc + cv.shape[1]
    rows, rank = qf.shape
    own = rank // nr
    share = own // nz if (own // nz) % 16 == 0 else own
    any_spec = pl.BlockSpec(memory_space=pltpu.HBM)
    vmem = pl.BlockSpec(memory_space=pltpu.VMEM)
    dma = pltpu.SemaphoreType.DMA
    shape = jax.ShapeDtypeStruct
    return pl.pallas_call(
        functools.partial(exchange, nz, nr),
        out_shape=(
            shape((width, cols), BF),
            shape((2, width, rank), BF),
            shape((rank, cols), BF),
            shape((own, cols), F32),
            shape((8, 128), F32),
        ),
        in_specs=[any_spec] * 11,
        out_specs=(any_spec, vmem, vmem, vmem, vmem),
        scratch_shapes=[
            pltpu.VMEM((tokens, width), BF),
            pltpu.VMEM(cq.shape, BF),
            pltpu.VMEM(cv.shape, BF),
            pltpu.VMEM((rows, cols), F32),
            pltpu.VMEM((rows, cols), BF),
            pltpu.VMEM((2, tokens, rank), BF),
            pltpu.VMEM((rank, cols), BF),
            pltpu.VMEM((nr - 1, own, cols), BF),
            pltpu.VMEM((nz, share, cols), BF),
            pltpu.VMEM((own, cols), BF),
            pltpu.VMEM((own, cols), BF),
            pltpu.VMEM((own, cols), F32),
            pltpu.VMEM((own, cols), F32),
            pltpu.VMEM((2, 8, 128), F32),
            dma((11,)),
            dma((nz - 1,)),
            dma((nz - 1,)),
            dma((nz - 1,)),
            dma((nz - 1,)),
            dma(((nz - 1) * (nr - 1),)),
            dma(((nz - 1) * (nr - 1),)),
            dma((nz - 1, 4)),
            dma((nz - 1, 4)),
            dma((nr - 1,)),
            dma((nr - 1,)),
            dma((nz - 1,)),
            dma((nz - 1,)),
            dma((nz - 1,)),
            dma((nz - 1,)),
            dma((nr - 1,)),
            dma((nr - 1,)),
            dma((3,)),
            dma((3,)),
        ],
        compiler_params=pltpu.CompilerParams(
            collective_id=0, has_side_effects=True, vmem_limit_bytes=60 * 1024 * 1024
        ),
    )(x, cq, cv, wq, wv, qf, vf, q1, q2, v1, v2)


def finish(
    f_ref,
    ratio_ref,
    scale_ref,
    w_ref,
    wq_ref,
    wv_ref,
    qf_ref,
    vf_ref,
    proj_ref,
    q1_ref,
    q2_ref,
    v1_ref,
    v2_ref,
    qd_out,
    vd_out,
    qm_out,
    vm_out,
    q1_out,
    q2_out,
    v1_out,
    v2_out,
    qcopy_out,
    vcopy_out,
):
    qc = wq_ref.shape[1]
    sets = (
        (0, pl.ds(0, qc), wq_ref, qf_ref, q1_ref, q2_ref, qd_out, qm_out, q1_out, q2_out, qcopy_out),
        (
            1,
            pl.ds(qc, wv_ref.shape[1]),
            wv_ref,
            vf_ref,
            v1_ref,
            v2_ref,
            vd_out,
            vm_out,
            v1_out,
            v2_out,
            vcopy_out,
        ),
    )
    for n, at, w, f, m1, m2, d_out, m_out, m1_out, m2_out, c_out in sets:
        scale = scale_ref[n : n + 1, 0:1]
        ratio = ratio_ref[:, at]
        raw = jnp.dot(f_ref[n], ratio, preferred_element_type=F32)
        c_out[...] = (w_ref[:, at].astype(F32) - RATE * (raw * scale)).astype(BF)
        d = jnp.dot(f[...], ratio, preferred_element_type=F32) * scale
        d_out[...] = d
        m_out[...] = w[...] - RATE * d
        m1_out[...], m2_out[...], _ = moments(proj_ref[:, at], m1[...], m2[...])


def run_finish(factors, ratio, scale, weights, wq, wv, qf, vf, proj, q1, q2, v1, v2):
    rows, qc = wq.shape
    vc = wv.shape[1]
    width, cols = weights.shape
    rank, own = qf.shape[1], q1.shape[0]
    steps = 8 if rows % 128 == 0 else 4

    def tall(n, c):
        return pl.BlockSpec((n // steps, c), lambda i: (i, 0))

    def whole(a):
        return pl.BlockSpec(a.shape, lambda i: (0,) * a.ndim)

    shape = jax.ShapeDtypeStruct
    return pl.pallas_call(
        finish,
        grid=(steps,),
        in_specs=[
            pl.BlockSpec((2, width // steps, rank), lambda i: (0, i, 0)),
            whole(ratio),
            whole(scale),
            tall(width, cols),
            tall(rows, qc),
            tall(rows, vc),
            tall(rows, rank),
            tall(rows, rank),
            tall(own, cols),
            tall(own, qc),
            tall(own, qc),
            tall(own, vc),
            tall(own, vc),
        ],
        out_specs=[
            tall(rows, qc),
            tall(rows, vc),
            tall(rows, qc),
            tall(rows, vc),
            tall(own, qc),
            tall(own, qc),
            tall(own, vc),
            tall(own, vc),
            tall(width, qc),
            tall(width, vc),
        ],
        out_shape=[
            shape((rows, qc), F32),
            shape((rows, vc), F32),
            shape((rows, qc), F32),
            shape((rows, vc), F32),
            shape((own, qc), F32),
            shape((own, qc), F32),
            shape((own, vc), F32),
            shape((own, vc), F32),
            shape((width, qc), BF),
            shape((width, vc), BF),
        ],
        compiler_params=pltpu.CompilerParams(vmem_limit_bytes=60 * 1024 * 1024),
    )(factors, ratio, scale, weights, wq, wv, qf, vf, proj, q1, q2, v1, v2)


def local(nz, nr, *args):
    _, _, _, wq, wv, qf, vf, q1, q2, v1, v2 = args
    weights, factors, ratio, proj, scale = run_exchange(nz, nr, *args)
    return tuple(
        run_finish(factors, ratio, scale, weights, wq, wv, qf, vf, proj, q1, q2, v1, v2)
    )


def solution(mesh):
    return jax.shard_map(
        functools.partial(local, mesh.shape["fs"], mesh.shape["rep"]),
        mesh=mesh,
        in_specs=(
            P(("fs", "rep"), None),
            P(("fs", "rep"), "tp"),
            P(("fs", "rep"), "tp"),
            P("fs", "tp"),
            P("fs", "tp"),
            P("fs", None),
            P("fs", None),
            P("rep", "tp"),
            P("rep", "tp"),
            P("rep", "tp"),
            P("rep", "tp"),
        ),
        out_specs=(
            P("fs", "tp"),
            P("fs", "tp"),
            P("fs", "tp"),
            P("fs", "tp"),
            P("rep", "tp"),
            P("rep", "tp"),
            P("rep", "tp"),
            P("rep", "tp"),
            P(None, "tp"),
            P(None, "tp"),
        ),
        check_vma=False,
    )
```

profile of v0, /device:TPU:0, one launch (start us, length us, event | category | flops | bytes accessed | tf_op | source)
XLA Modules:
  0.0 100.7 jit_solution(9465584938906942862)
XLA Ops:
  0.6 87.1 %shard_map.186 = (bf16[2048,1536]{1,0:T(8,128)(2,1)}, bf16[2,2048,256]{2,1,0:T(8,128)(2,1)}, bf16[256,1536]{1,0:T(8,128)(2,1)}, f32[64,1536]{1,0:T(8,128)}, f32[8,128]{1,0:T(8,128)}) custom-call(bf16[768,2048]{1,0:T(8,128)(2,1)} %x_hbm.1, bf16[768,512]{1,0:T(8,128)(2,1)} %cq_hbm.1, bf16[768,1024]{1,0:T(8,128)(2,1)} %cv_hbm.1, f32[512,512]{1,0:T(8,128)} %wq_ref.1, ...), custom_call_target="tpu_custom_call" | custom-call | tf_op jit(solution)/shard_map/pallas_call | solution.py:371
  87.8 12.9 %shard_map.187 = (f32[512,512]{1,0:T(8,128)}, f32[512,1024]{1,0:T(8,128)}, f32[512,512]{1,0:T(8,128)}, f32[512,1024]{1,0:T(8,128)}, f32[64,512]{1,0:T(8,128)}, /...) custom-call(bf16[2,2048,256]{2,1,0:T(8,128)(2,1)} %get-tuple-element, ...), custom_call_target="tpu_custom_call" | custom-call | tf_op jit(solution)/shard_map/pallas_call | solution.py:490
where the time goes:
time: 101 us
  Pallas kernels  100 us (99%)
    pallas_call x1, Pallas kernels, run_exchange(): pl.pallas_call(functools.partial(exchange, nz, nr), out_shape=(shape((wid...  87.1 us
    pallas_call x1, Pallas kernels, run_finish(): pl.pallas_call(finish, grid=(steps,), in_specs=[pl.BlockSpec((2, width //...  12.9 us

commit v1 on v0

--- a/solution.py
+++ b/solution.py
@@ -533,8 +533,508 @@
     )(factors, ratio, scale, weights, wq, wv, qf, vf, proj, q1, q2, v1, v2)
 
 
+def line_exchange(
+    quarter,
+    chunks,
+    x_hbm,
+    cq_hbm,
+    cv_hbm,
+    wq_hbm,
+    wv_hbm,
+    qf_hbm,
+    vf_hbm,
+    q1_hbm,
+    q2_hbm,
+    v1_hbm,
+    v2_hbm,
+    w_ref,
+    f_ref,
+    ratio_ref,
+    wf_ref,
+    m1_out,
+    m2_out,
+    scale_out,
+    x_ref,
+    cq_ref,
+    cv_ref,
+    acc_ref,
+    low_ref,
+    part_ref,
+    rs_ref,
+    zs_ref,
+    z_ref,
+    zh_ref,
+    m1_ref,
+    m2_ref,
+    g_ref,
+    sq_ref,
+    local_sem,
+    fz_s,
+    fz_r,
+    fp_s,
+    fp_r,
+    wz_s,
+    wz_r,
+    wp_s,
+    wp_r,
+    rs_s,
+    rs_r,
+    zs_s,
+    zs_r,
+    zg_s,
+    zg_r,
+    ag_s,
+    ag_r,
+    tp_s,
+    tp_r,
+):
+    z = lax.axis_index("fs")
+    r = lax.axis_index("rep")
+    t = lax.axis_index("tp")
+    nz, nr = 4, 4
+    rows = qf_hbm.shape[0]
+    part = rows // nr
+    qc = cq_ref.shape[1]
+    width, cols = w_ref.shape
+    half = cols // 2
+    rank = low_ref.shape[2]
+    own = rank // nr
+    share = own // nz
+    tokens = x_ref.shape[0]
+    side = r + 1 - 2 * lax.rem(r, 2)
+    over = lax.rem(r + 2, nr)
+    corner = nr - 1 - r
+    other = 1 - t
+    peer = {1: side, 2: over, 3: corner}
+    upper = lax.div(z, 2)
+    near = z + 1 - 2 * lax.rem(z, 2)
+    mid = 2 - upper
+    far = 3 - 3 * upper
+    planes = [near, mid, far]
+    sent = []
+
+    def remote(src, dst, ss, rs, dev):
+        return pltpu.make_async_remote_copy(
+            src_ref=src,
+            dst_ref=dst,
+            send_sem=ss,
+            recv_sem=rs,
+            device_id=dev,
+            device_id_type=pl.DeviceIdType.MESH,
+        )
+
+    def send(src, dst, ss, rs, dev):
+        c = remote(src, dst, ss, rs, dev)
+        c.start()
+        sent.append(c)
+        return c
+
+    def arrive(dst, rs):
+        remote(dst, dst, tp_s.at[0], rs, (z, r, other)).wait_recv()
+
+    def at(start, size, step):
+        return pl.ds(pl.multiple_of(start, step), size)
+
+    def fac_copy(src):
+        return pltpu.make_async_copy(src, f_ref.at[t, at(z * rows, rows, rows)], local_sem.at[0])
+
+    @pl.when(t == 0)
+    def _():
+        fac_copy(qf_hbm).start()
+
+    @pl.when(t == 1)
+    def _():
+        fac_copy(vf_hbm).start()
+
+    left, right = pl.ds(0, qc), pl.ds(qc, cols - qc)
+    wq_in = pltpu.make_async_copy(wq_hbm, wf_ref.at[:, left], local_sem.at[1])
+    wv_in = pltpu.make_async_copy(wv_hbm, wf_ref.at[:, right], local_sem.at[2])
+    x_in = pltpu.make_async_copy(x_hbm, x_ref, local_sem.at[3])
+    cq_in = pltpu.make_async_copy(cq_hbm, cq_ref, local_sem.at[4])
+    cv_in = pltpu.make_async_copy(cv_hbm, cv_ref, local_sem.at[5])
+    mom = [
+        pltpu.make_async_copy(src, dst.at[:, span], local_sem.at[6 + n])
+        for n, (src, dst, span) in enumerate(
+            (
+                (q1_hbm, m1_ref, left),
+                (v1_hbm, m1_ref, right),
+                (q2_hbm, m2_ref, left),
+                (v2_hbm, m2_ref, right),
+            )
+        )
+    ]
+    for c in [wq_in, wv_in, x_in, cq_in, cv_in] + mom:
+        c.start()
+
+    barrier = pltpu.get_barrier_semaphore()
+    peers = [(p, r, t) for p in planes]
+    peers += [(z, peer[j], t) for j in peer]
+    peers += [(z, r, other)]
+    for dev in peers:
+        pl.semaphore_signal(
+            barrier, inc=1, device_id=dev, device_id_type=pl.DeviceIdType.MESH
+        )
+    pl.semaphore_wait(barrier, len(peers))
+
+    def fac_rows(plane, rr):
+        return f_ref.at[t, at(plane * rows + rr * part, part, part)]
+
+    fac_copy(qf_hbm).wait()
+    for i, p in enumerate(planes):
+        here = fac_rows(z, r)
+        send(here, here, fz_s.at[i], fz_r.at[z], (p, r, t))
+
+    offsets = [sum(chunks[:c]) for c in range(len(chunks))]
+
+    def w_rows(plane, rr, c):
+        return w_ref.at[at(plane * rows + rr * quarter + offsets[c], chunks[c], 16)]
+
+    def w_rest(plane):
+        return w_ref.at[at(plane * rows + nr * quarter, rows - nr * quarter, 16)]
+
+    wq_in.wait()
+    wv_in.wait()
+    w_ref[at(z * rows, rows, rows), :] = wf_ref[...].astype(BF)
+
+    def w_line(i, c):
+        here = w_rows(z, r, c)
+        send(here, here, wz_s.at[i, c], wz_r.at[z, c], (planes[i], r, t))
+
+    def w_line_rest(i):
+        here = w_rest(z)
+        n = len(chunks)
+        send(here, here, wz_s.at[i, n], wz_r.at[z, n], (planes[i], r, t))
+
+    for i in range(3):
+        for c in range(len(chunks)):
+            w_line(i, c)
+
+    def spread(i, c):
+        there = w_rows(planes[i], r, c)
+        arrive(there, wz_r.at[planes[i], c])
+        for n, dev in ((0, side), (1, over)):
+            send(there, there, wp_s.at[i, c, n], wp_r.at[i, c, n], (z, dev, t))
+
+    def relay(i, c):
+        for n, src, dev, begin in ((0, side, over, 0), (1, over, side, half)):
+            whole = w_rows(planes[i], src, c)
+            arrive(whole, wp_r.at[i, c, n])
+            there = whole.at[:, pl.ds(begin, half)]
+            send(there, there, wp_s.at[i, c, 2 + n], wp_r.at[i, c, 2 + n], (z, dev, t))
+
+    def low_add(plane, first):
+        tile = tokens // 3
+
+        @pl.loop(0, 3)
+        def _(n):
+            span = at(n * tile, tile, 16)
+            a = jnp.dot(
+                x_ref[span, at(plane * rows, rows, rows)],
+                f_ref[t, at(plane * rows, rows, rows)],
+                preferred_element_type=F32,
+            )
+            acc_ref[span, :] = a if first else acc_ref[span, :] + a
+
+    def fac_spread(i):
+        there = fac_rows(planes[i], r)
+        arrive(there, fz_r.at[planes[i]])
+        for j in (3, 1, 2):
+            send(there, there, fp_s.at[i, j - 1], fp_r.at[i, j - 1], (z, peer[j], t))
+
+    def fac_gather(i):
+        for j in (1, 2, 3):
+            arrive(fac_rows(planes[i], peer[j]), fp_r.at[i, j - 1])
+        low_add(planes[i], False)
+
+    x_in.wait()
+    low_add(z, True)
+    fac_spread(0)
+    fac_spread(1)
+    fac_spread(2)
+    spread(0, 0)
+    fac_gather(0)
+    spread(0, 1)
+    fac_gather(1)
+    fac_gather(2)
+    low_ref[t] = acc_ref[...].astype(BF)
+    send(low_ref.at[t], low_ref.at[t], tp_s.at[1], tp_r.at[1], (z, r, other))
+    fx = send(f_ref.at[t], f_ref.at[t], tp_s.at[0], tp_r.at[0], (z, r, other))
+    cq_in.wait()
+    cv_in.wait()
+    arrive(low_ref.at[other], tp_r.at[1])
+    dims = (((0,), (0,)), ((), ()))
+    part_ref[:, :qc] = lax.dot_general(
+        low_ref[0], cq_ref[...], dims, preferred_element_type=F32
+    ).astype(BF)
+    part_ref[:, qc:] = lax.dot_general(
+        low_ref[1], cv_ref[...], dims, preferred_element_type=F32
+    ).astype(BF)
+
+    def low_rows(rr, plane):
+        return at(rr * own + plane * share, share, share)
+
+    def share_rows(plane):
+        return at(plane * share, share, share)
+
+    order = [far, mid, near, z]
+    for i, p in enumerate(order):
+        for j in (3, 1, 2):
+            send(
+                part_ref.at[low_rows(peer[j], p)],
+                rs_ref.at[j - 1, share_rows(p)],
+                rs_s.at[i, j - 1],
+                rs_r.at[i, j - 1],
+                (z, peer[j], t),
+            )
+    relay(0, 0)
+    relay(0, 1)
+
+    def collect(i, p):
+        for j in (1, 2, 3):
+            arrive(rs_ref.at[j - 1, share_rows(p)], rs_r.at[i, j - 1])
+        total = part_ref[low_rows(r, p), :].astype(F32)
+        for j in (1, 2, 3):
+            total = total + rs_ref[j - 1, share_rows(p), :].astype(F32)
+        return total
+
+    for i, p in enumerate(order[:3]):
+        zs_ref[share_rows(p), :] = collect(i, p).astype(BF)
+        send(zs_ref.at[share_rows(p)], z_ref.at[z], zs_s.at[i], zs_r.at[z], (p, r, t))
+    spread(1, 0)
+    proj = collect(3, z)
+    w_line_rest(0)
+    for c in mom:
+        c.wait()
+    for p in planes:
+        arrive(z_ref.at[p], zs_r.at[p])
+        proj = proj + z_ref[p].astype(F32)
+    zh_ref[share_rows(z), :] = proj.astype(BF)
+    for i, p in ((2, far), (1, mid), (0, near)):
+        here = zh_ref.at[share_rows(z)]
+        send(here, here, zg_s.at[i], zg_r.at[z], (p, r, t))
+
+    def ratios(i, p):
+        span = share_rows(p)
+        first, second, ratio = moments(
+            zh_ref[span, :].astype(F32), m1_ref[span, :], m2_ref[span, :]
+        )
+        m1_out[span, :] = first
+        m2_out[span, :] = second
+        ratio_ref[low_rows(r, p), :] = ratio.astype(BF)
+        here = ratio_ref.at[low_rows(r, p)]
+        for j in (3, 1, 2):
+            send(here, here, ag_s.at[i, j - 1], ag_r.at[i, j - 1], (z, peer[j], t))
+
+    ratios(0, z)
+    w_line_rest(1)
+    w_line_rest(2)
+    for i, p in enumerate(planes):
+        arrive(zh_ref.at[share_rows(p)], zg_r.at[p])
+        ratios(1 + i, p)
+    spread(1, 1)
+    relay(1, 0)
+    spread(2, 0)
+    spread(2, 1)
+    arrive(f_ref.at[other], tp_r.at[0])
+    for n in range(2):
+        g = lax.dot_general(f_ref[n], f_ref[n], dims, preferred_element_type=F32)
+        top = g.astype(BF)
+        g_ref[n, 0] = top
+        g_ref[n, 1] = (g - top.astype(F32)).astype(BF)
+    relay(1, 1)
+    for i, p in enumerate([z] + planes):
+        for j in (1, 2, 3):
+            arrive(ratio_ref.at[low_rows(peer[j], p)], ag_r.at[i, j - 1])
+    relay(2, 0)
+    relay(2, 1)
+
+    def squares(n, span):
+        ratio = ratio_ref[:, span]
+        a = jnp.dot(g_ref[n, 0], ratio, preferred_element_type=F32)
+        a = a + jnp.dot(g_ref[n, 1], ratio, preferred_element_type=F32)
+        a = jnp.sum(a * ratio.astype(F32), axis=0, keepdims=True)
+        return jnp.sum(a, axis=1, keepdims=True)
+
+    qs = squares(0, slice(0, qc)) / (width * qc * 2)
+    vs = squares(1, slice(qc, cols)) / (width * (cols - qc) * 2)
+    line = lax.broadcasted_iota(jnp.int32, sq_ref.shape[1:], 0)
+    sq_ref[t] = jnp.where(line == 0, qs, vs)
+    send(sq_ref.at[t], sq_ref.at[t], tp_s.at[2], tp_r.at[2], (z, r, other))
+    arrive(sq_ref.at[other], tp_r.at[2])
+    scale_out[...] = lax.rsqrt(jnp.maximum(sq_ref[0] + sq_ref[1], 0.0) + EPS_NORM)
+    for i, p in enumerate(planes):
+        arrive(w_rest(p), wz_r.at[p, len(chunks)])
+        for c in range(len(chunks)):
+            for n, begin in ((2, 0), (3, half)):
+                arrive(w_rows(p, corner, c).at[:, pl.ds(begin, half)], wp_r.at[i, c, n])
+    for c in sent:
+        c.wait_send()
+
+
+def run_line_exchange(x, cq, cv, wq, wv, qf, vf, q1, q2, v1, v2):
+    tokens, width = x.shape
+    qc = cq.shape[1]
+    cols = qc + cv.shape[1]
+    rows, rank = qf.shape
+    own = rank // 4
+    share = own // 4
+    quarter = rows // 4 // 128 * 112
+    chunks = (quarter // 32 * 16, quarter - quarter // 32 * 16)
+    any_spec = pl.BlockSpec(memory_space=pltpu.HBM)
+    vmem = pl.BlockSpec(memory_space=pltpu.VMEM)
+    dma = pltpu.SemaphoreType.DMA
+    n = len(chunks)
+    return pl.pallas_call(
+        functools.partial(line_exchange, quarter, chunks),
+        out_shape=(
+            pltpu.VMEM((width, cols), BF),
+            pltpu.VMEM((2, width, rank), BF),
+            pltpu.VMEM((rank, cols), BF),
+            pltpu.VMEM((rows, cols), F32),
+            pltpu.VMEM((own, cols), F32),
+            pltpu.VMEM((own, cols), F32),
+            pltpu.VMEM((8, 128), F32),
+        ),
+        in_specs=[any_spec] * 11,
+        out_specs=(vmem,) * 7,
+        scratch_shapes=[
+            pltpu.VMEM((tokens, width), BF),
+            pltpu.VMEM(cq.shape, BF),
+            pltpu.VMEM(cv.shape, BF),
+            pltpu.VMEM((tokens, rank), F32),
+            pltpu.VMEM((2, tokens, rank), BF),
+            pltpu.VMEM((rank, cols), BF),
+            pltpu.VMEM((3, own, cols), BF),
+            pltpu.VMEM((own, cols), BF),
+            pltpu.VMEM((4, share, cols), BF),
+            pltpu.VMEM((own, cols), BF),
+            pltpu.VMEM((own, cols), F32),
+            pltpu.VMEM((own, cols), F32),
+            pltpu.VMEM((2, 2, rank, rank), BF),
+            pltpu.VMEM((2, 8, 128), F32),
+            dma((10,)),
+            dma((3,)),
+            dma((4,)),
+            dma((3, 3)),
+            dma((3, 3)),
+            dma((3, n + 1)),
+            dma((4, n + 1)),
+            dma((3, n, 4)),
+            dma((3, n, 4)),
+            dma((4, 3)),
+            dma((4, 3)),
+            dma((3,)),
+            dma((4,)),
+            dma((3,)),
+            dma((4,)),
+            dma((4, 3)),
+            dma((4, 3)),
+            dma((3,)),
+            dma((3,)),
+        ],
+        compiler_params=pltpu.CompilerParams(
+            collective_id=0, has_side_effects=True, vmem_limit_bytes=48 * 1024 * 1024
+        ),
+    )(x, cq, cv, wq, wv, qf, vf, q1, q2, v1, v2)
+
+
+def line_finish(
+    steps,
+    w_ref,
+    f_ref,
+    ratio_ref,
+    wf_ref,
+    m1_ref,
+    m2_ref,
+    scale_ref,
+    qd_out,
+    vd_out,
+    qm_out,
+    vm_out,
+    q1_out,
+    q2_out,
+    v1_out,
+    v2_out,
+    qcopy_out,
+    vcopy_out,
+):
+    i = pl.program_id(0)
+    z = lax.axis_index("fs")
+    rows, cols = wf_ref.shape
+    qc = qd_out.shape[1]
+    tall, small, low = w_ref.shape[0] // steps, rows // steps, m1_ref.shape[0] // steps
+    every = pl.ds(pl.multiple_of(i * tall, tall), tall)
+    mine = pl.ds(pl.multiple_of(z * rows + i * small, small), small)
+    here = pl.ds(pl.multiple_of(i * small, small), small)
+    moment = pl.ds(pl.multiple_of(i * low, low), low)
+    sets = (
+        (0, slice(0, qc), qd_out, qm_out, q1_out, q2_out, qcopy_out),
+        (1, slice(qc, cols), vd_out, vm_out, v1_out, v2_out, vcopy_out),
+    )
+    for n, at, d_out, m_out, m1_out, m2_out, c_out in sets:
+        scale = scale_ref[n : n + 1, 0:1]
+        ratio = ratio_ref[:, at]
+        d = jnp.dot(f_ref[n, mine], ratio, preferred_element_type=F32) * scale
+        d_out[...] = d
+        m_out[...] = wf_ref[here, at] - RATE * d
+        m1_out[...] = m1_ref[moment, at]
+        m2_out[...] = m2_ref[moment, at]
+        raw = jnp.dot(f_ref[n, every], ratio, preferred_element_type=F32)
+        c_out[...] = (w_ref[every, at].astype(F32) - RATE * (raw * scale)).astype(BF)
+
+
+def run_line_finish(weights, factors, ratio, wf, m1, m2, scale, qc):
+    rows, cols = wf.shape
+    vc = cols - qc
+    width, own = weights.shape[0], m1.shape[0]
+    steps = 8
+
+    def tall(n, c):
+        return pl.BlockSpec((n // steps, c), lambda i: (i, 0))
+
+    shape = jax.ShapeDtypeStruct
+    return pl.pallas_call(
+        functools.partial(line_finish, steps),
+        grid=(steps,),
+        in_specs=[pl.BlockSpec(memory_space=pltpu.VMEM)] * 7,
+        out_specs=[
+            tall(rows, qc),
+            tall(rows, vc),
+            tall(rows, qc),
+            tall(rows, vc),
+            tall(own, qc),
+            tall(own, qc),
+            tall(own, vc),
+            tall(own, vc),
+            tall(width, qc),
+            tall(width, vc),
+        ],
+        out_shape=[
+            shape((rows, qc), F32),
+            shape((rows, vc), F32),
+            shape((rows, qc), F32),
+            shape((rows, vc), F32),
+            shape((own, qc), F32),
+            shape((own, qc), F32),
+            shape((own, vc), F32),
+            shape((own, vc), F32),
+            shape((width, qc), BF),
+            shape((width, vc), BF),
+        ],
+        compiler_params=pltpu.CompilerParams(vmem_limit_bytes=24 * 1024 * 1024),
+    )(weights, factors, ratio, wf, m1, m2, scale)
+
+
+def suits_line(nz, nr, qf, cq, cv):
+    rows, rank = qf.shape
+    cols = cq.shape[1] + cv.shape[1]
+    return nz == 4 and nr == 4 and rows % 512 == 0 and rank % 256 == 0 and cols % 256 == 0
+
+
 def local(nz, nr, *args):
-    _, _, _, wq, wv, qf, vf, q1, q2, v1, v2 = args
+    _, cq, cv, wq, wv, qf, vf, q1, q2, v1, v2 = args
+    if suits_line(nz, nr, qf, cq, cv):
+        return tuple(run_line_finish(*run_line_exchange(*args), cq.shape[1]))
     weights, factors, ratio, proj, scale = run_exchange(nz, nr, *args)
     return tuple(
         run_finish(factors, ratio, scale, weights, wq, wv, qf, vf, proj, q1, q2, v1, v2)

time: 101 us -> 91.2 us (0.903)
  the two profiles are of different devices: /device:TPU:0 before, /device:TPU:8 now
where the time goes in v1:
time: 91.2 us; the launch traced here: 91.1 us
  Pallas kernels  90.4 us (99%)
    pallas_call x1, Pallas kernels, run_line_exchange(): pl.pallas_call(functools.partial(line_exchange, quarter, chunks), out_sha...  83.5 us
    pallas_call x1, Pallas kernels, run_line_finish(): pl.pallas_call(functools.partial(line_finish, steps), grid=(steps,), in_s...  6.86 us

profile of v1, /device:TPU:8, one launch (start us, length us, event | category | flops | bytes accessed | tf_op | source)
XLA Modules:
  0.0 91.1 jit_solution(5218511505528445234)
XLA Ops:
  0.6 83.5 %shard_map.186 = (bf16[2048,1536]{1,0:T(8,128)(2,1)S(1)}, bf16[2,2048,256]{2,1,0:T(8,128)(2,1)S(1)}, bf16[256,1536]{1,0:T(8,128)(2,1)S(1)}, f32[512,1536]{1,0:T(...) custom-call(bf16[768,2048]{1,0:T(8,128)(2,1)} %x_hbm.1, ...), custom_call_target="tpu_custom_call" | custom-call | tf_op jit(solution)/shard_map/pallas_call | solution.py:887
  84.2 6.9 %shard_map.187 = (f32[512,512]{1,0:T(8,128)}, f32[512,1024]{1,0:T(8,128)}, f32[512,512]{1,0:T(8,128)}, f32[512,1024]{1,0:T(8,128)}, f32[64,512]{1,0:T(8,128)}, /...) custom-call(bf16[2048,1536]{1,0:T(8,128)(2,1)S(1)} %get-tuple-elemen, ...), custom_call_target="tpu_custom_call" | custom-call | tf_op jit(solution)/shard_map/pallas_call | solution.py:996

commit v2 on v1

--- a/solution.py
+++ b/solution.py
@@ -536,6 +536,7 @@
 def line_exchange(
     quarter,
     chunks,
+    rests,
     x_hbm,
     cq_hbm,
     cv_hbm,
@@ -560,8 +561,11 @@
     acc_ref,
     low_ref,
     part_ref,
-    rs_ref,
+    ra_ref,
+    tb_ref,
+    rb_ref,
     zs_ref,
+    zo_ref,
     z_ref,
     zh_ref,
     m1_ref,
@@ -577,8 +581,10 @@
     wz_r,
     wp_s,
     wp_r,
-    rs_s,
-    rs_r,
+    ra_s,
+    ra_r,
+    rb_s,
+    rb_r,
     zs_s,
     zs_r,
     zg_s,
@@ -601,17 +607,18 @@
     own = rank // nr
     share = own // nz
     tokens = x_ref.shape[0]
-    side = r + 1 - 2 * lax.rem(r, 2)
+    px, py = lax.rem(r, 2), lax.div(r, 2)
+    side = r + 1 - 2 * px
     over = lax.rem(r + 2, nr)
     corner = nr - 1 - r
     other = 1 - t
-    peer = {1: side, 2: over, 3: corner}
     upper = lax.div(z, 2)
     near = z + 1 - 2 * lax.rem(z, 2)
     mid = 2 - upper
     far = 3 - 3 * upper
     planes = [near, mid, far]
-    sent = []
+    inner = jnp.logical_and(z > 0, z < nz - 1)
+    sent, passed = [], []
 
     def remote(src, dst, ss, rs, dev):
         return pltpu.make_async_remote_copy(
@@ -627,7 +634,14 @@
         c = remote(src, dst, ss, rs, dev)
         c.start()
         sent.append(c)
-        return c
+
+    def send_inner(src, dst, ss, rs, dev):
+        c = remote(src, dst, ss, rs, dev)
+        passed.append(c)
+
+        @pl.when(inner)
+        def _():
+            c.start()
 
     def arrive(dst, rs):
         remote(dst, dst, tp_s.at[0], rs, (z, r, other)).wait_recv()
@@ -668,7 +682,7 @@
 
     barrier = pltpu.get_barrier_semaphore()
     peers = [(p, r, t) for p in planes]
-    peers += [(z, peer[j], t) for j in peer]
+    peers += [(z, p, t) for p in (side, over, corner)]
     peers += [(z, r, other)]
     for dev in peers:
         pl.semaphore_signal(
@@ -676,6 +690,29 @@
         )
     pl.semaphore_wait(barrier, len(peers))
 
+    class Spread:
+        def __init__(self, view, split, ss, rs):
+            self.view, self.split, self.ss, self.rs = view, split, ss, rs
+
+        def start(self):
+            here = self.view(r)
+            for n, dev in ((0, side), (1, over)):
+                send(here, here, self.ss.at[n], self.rs.at[n], (z, dev, t))
+
+        def relay(self):
+            for n, src, dev in ((0, side, over), (1, over, side)):
+                whole = self.view(src)
+                arrive(whole, self.rs.at[n])
+                there = self.split(whole, n)
+                send(there, there, self.ss.at[2 + n], self.rs.at[2 + n], (z, dev, t))
+
+        def finish(self):
+            for n in range(2):
+                arrive(self.split(self.view(corner), n), self.rs.at[2 + n])
+
+    def halves(ref, n):
+        return ref.at[:, pl.ds(n * half, half)]
+
     def fac_rows(plane, rr):
         return f_ref.at[t, at(plane * rows + rr * part, part, part)]
 
@@ -684,43 +721,46 @@
         here = fac_rows(z, r)
         send(here, here, fz_s.at[i], fz_r.at[z], (p, r, t))
 
-    offsets = [sum(chunks[:c]) for c in range(len(chunks))]
+    spans = [(n, s, True) for n, s in zip([sum(chunks[:c]) for c in range(len(chunks))], chunks)]
+    spans += [(n, s, False) for n, s in zip([sum(rests[:c]) for c in range(len(rests))], rests)]
 
     def w_rows(plane, rr, c):
-        return w_ref.at[at(plane * rows + rr * quarter + offsets[c], chunks[c], 16)]
-
-    def w_rest(plane):
-        return w_ref.at[at(plane * rows + nr * quarter, rows - nr * quarter, 16)]
-
-    wq_in.wait()
-    wv_in.wait()
-    w_ref[at(z * rows, rows, rows), :] = wf_ref[...].astype(BF)
-
-    def w_line(i, c):
+        begin, size, split = spans[c]
+        begin = plane * rows + begin + (rr * quarter if split else nr * quarter)
+        return w_ref.at[at(begin, size, 8)]
+
+    def w_own(c):
         here = w_rows(z, r, c)
-        send(here, here, wz_s.at[i, c], wz_r.at[z, c], (planes[i], r, t))
-
-    def w_line_rest(i):
-        here = w_rest(z)
-        n = len(chunks)
-        send(here, here, wz_s.at[i, n], wz_r.at[z, n], (planes[i], r, t))
-
-    for i in range(3):
-        for c in range(len(chunks)):
-            w_line(i, c)
-
-    def spread(i, c):
-        there = w_rows(planes[i], r, c)
-        arrive(there, wz_r.at[planes[i], c])
-        for n, dev in ((0, side), (1, over)):
-            send(there, there, wp_s.at[i, c, n], wp_r.at[i, c, n], (z, dev, t))
-
-    def relay(i, c):
-        for n, src, dev, begin in ((0, side, over, 0), (1, over, side, half)):
-            whole = w_rows(planes[i], src, c)
-            arrive(whole, wp_r.at[i, c, n])
-            there = whole.at[:, pl.ds(begin, half)]
-            send(there, there, wp_s.at[i, c, 2 + n], wp_r.at[i, c, 2 + n], (z, dev, t))
+        send(here, here, wz_s.at[3, c], wz_r.at[z, c], (near, r, t))
+        send_inner(here, here, wz_s.at[4, c], wz_r.at[z, c], (mid, r, t))
+
+    def w_pass(i, c):
+        here = w_rows(planes[i], r, c)
+        to = near if i else mid
+        copy = remote(here, here, wz_s.at[i, c], wz_r.at[planes[i], c], (to, r, t))
+        passed.append(copy)
+
+        @pl.when(inner)
+        def _():
+            arrive(here, wz_r.at[planes[i], c])
+            copy.start()
+
+    def w_land(i, c):
+        @pl.when(jnp.logical_not(inner))
+        def _():
+            arrive(w_rows(planes[i], r, c), wz_r.at[planes[i], c])
+
+    def w_start(i, c):
+        w_land(i, c)
+        w_in[i][c].start()
+
+    w_in = [
+        [
+            Spread(functools.partial(lambda p, c, rr: w_rows(p, rr, c), p, c), halves, wp_s.at[i, c], wp_r.at[i, c])
+            for c in range(len(chunks))
+        ]
+        for i, p in enumerate(planes)
+    ]
 
     def low_add(plane, first):
         tile = tokens // 3
@@ -735,85 +775,92 @@
             )
             acc_ref[span, :] = a if first else acc_ref[span, :] + a
 
-    def fac_spread(i):
-        there = fac_rows(planes[i], r)
-        arrive(there, fz_r.at[planes[i]])
-        for j in (3, 1, 2):
-            send(there, there, fp_s.at[i, j - 1], fp_r.at[i, j - 1], (z, peer[j], t))
-
-    def fac_gather(i):
-        for j in (1, 2, 3):
-            arrive(fac_rows(planes[i], peer[j]), fp_r.at[i, j - 1])
+    fac = [
+        Spread(
+            functools.partial(fac_rows, p),
+            lambda ref, n: ref.at[pl.ds(n * (part // 2), part // 2)],
+            fp_s.at[i],
+            fp_r.at[i],
+        )
+        for i, p in enumerate(planes)
+    ]
+
+    def fac_start(i):
+        arrive(fac_rows(planes[i], r), fz_r.at[planes[i]])
+        fac[i].start()
+
+    def fac_finish(i):
+        fac[i].finish()
         low_add(planes[i], False)
 
-    x_in.wait()
-    low_add(z, True)
-    fac_spread(0)
-    fac_spread(1)
-    fac_spread(2)
-    spread(0, 0)
-    fac_gather(0)
-    spread(0, 1)
-    fac_gather(1)
-    fac_gather(2)
-    low_ref[t] = acc_ref[...].astype(BF)
-    send(low_ref.at[t], low_ref.at[t], tp_s.at[1], tp_r.at[1], (z, r, other))
-    fx = send(f_ref.at[t], f_ref.at[t], tp_s.at[0], tp_r.at[0], (z, r, other))
-    cq_in.wait()
-    cv_in.wait()
-    arrive(low_ref.at[other], tp_r.at[1])
-    dims = (((0,), (0,)), ((), ()))
-    part_ref[:, :qc] = lax.dot_general(
-        low_ref[0], cq_ref[...], dims, preferred_element_type=F32
-    ).astype(BF)
-    part_ref[:, qc:] = lax.dot_general(
-        low_ref[1], cv_ref[...], dims, preferred_element_type=F32
-    ).astype(BF)
+    def share_rows(plane):
+        return at(plane * share, share, share)
 
     def low_rows(rr, plane):
         return at(rr * own + plane * share, share, share)
 
-    def share_rows(plane):
-        return at(plane * share, share, share)
-
+    lo, hi = pl.ds(0, half), pl.ds(half, half)
     order = [far, mid, near, z]
-    for i, p in enumerate(order):
-        for j in (3, 1, 2):
-            send(
-                part_ref.at[low_rows(peer[j], p)],
-                rs_ref.at[j - 1, share_rows(p)],
-                rs_s.at[i, j - 1],
-                rs_r.at[i, j - 1],
-                (z, peer[j], t),
-            )
-    relay(0, 0)
-    relay(0, 1)
-
-    def collect(i, p):
-        for j in (1, 2, 3):
-            arrive(rs_ref.at[j - 1, share_rows(p)], rs_r.at[i, j - 1])
-        total = part_ref[low_rows(r, p), :].astype(F32)
-        for j in (1, 2, 3):
-            total = total + rs_ref[j - 1, share_rows(p), :].astype(F32)
-        return total
-
-    for i, p in enumerate(order[:3]):
-        zs_ref[share_rows(p), :] = collect(i, p).astype(BF)
-        send(zs_ref.at[share_rows(p)], z_ref.at[z], zs_s.at[i], zs_r.at[z], (p, r, t))
-    spread(1, 0)
-    proj = collect(3, z)
-    w_line_rest(0)
-    for c in mom:
-        c.wait()
-    for p in planes:
-        arrive(z_ref.at[p], zs_r.at[p])
-        proj = proj + z_ref[p].astype(F32)
-    zh_ref[share_rows(z), :] = proj.astype(BF)
-    for i, p in ((2, far), (1, mid), (0, near)):
+
+    def sum_start(i):
+        span = share_rows(order[i])
+        for n, src, dev in (
+            (0, part_ref.at[:, 1 - px, span, lo], side),
+            (1, part_ref.at[1 - py, :, span, hi], over),
+        ):
+            send(src, ra_ref.at[n, :, span], ra_s.at[i, n], ra_r.at[i, n], (z, dev, t))
+
+    def sum_relay(i):
+        span = share_rows(order[i])
+        for n in range(2):
+            arrive(ra_ref.at[n, :, span], ra_r.at[i, n])
+        for n, mine, theirs, dev in (
+            (0, part_ref[1 - py, px, span, lo], ra_ref[0, 1 - py, span, :], over),
+            (1, part_ref[py, 1 - px, span, hi], ra_ref[1, 1 - px, span, :], side),
+        ):
+            tb_ref[n, span, :] = (mine.astype(F32) + theirs.astype(F32)).astype(BF)
+            send(tb_ref.at[n, span], rb_ref.at[n, span], rb_s.at[i, n], rb_r.at[i, n], (z, dev, t))
+
+    def sum_finish(i):
+        span = share_rows(order[i])
+        for n in range(2):
+            arrive(rb_ref.at[n, span], rb_r.at[i, n])
+        out = []
+        for n, cut, theirs in ((0, lo, ra_ref[0, py, span, :]), (1, hi, ra_ref[1, px, span, :])):
+            a = part_ref[py, px, span, cut].astype(F32) + theirs.astype(F32)
+            out.append(a + rb_ref[n, span, :].astype(F32))
+        if i == 3:
+            zo_ref[:, lo], zo_ref[:, hi] = out
+        else:
+            zs_ref[span, lo] = out[0].astype(BF)
+            zs_ref[span, hi] = out[1].astype(BF)
+            send(zs_ref.at[span], z_ref.at[z], zs_s.at[i], zs_r.at[z], (order[i], r, t))
+
+    def line_sum():
+        proj = zo_ref[...]
+        for p in planes:
+            arrive(z_ref.at[p], zs_r.at[p])
+            proj = proj + z_ref[p].astype(F32)
         here = zh_ref.at[share_rows(z)]
-        send(here, here, zg_s.at[i], zg_r.at[z], (p, r, t))
-
-    def ratios(i, p):
+        zh_ref[share_rows(z), :] = proj.astype(BF)
+        for i, p in ((2, far), (1, mid), (0, near)):
+            send(here, here, zg_s.at[i], zg_r.at[z], (p, r, t))
+
+    ratio_in = [
+        Spread(
+            functools.partial(lambda p, rr: ratio_ref.at[low_rows(rr, p)], p),
+            halves,
+            ag_s.at[i],
+            ag_r.at[i],
+        )
+        for i, p in enumerate([z] + planes)
+    ]
+
+    def ratio_start(i):
+        p = z
+        if i:
+            p = planes[i - 1]
+            arrive(zh_ref.at[share_rows(p)], zg_r.at[p])
         span = share_rows(p)
         first, second, ratio = moments(
             zh_ref[span, :].astype(F32), m1_ref[span, :], m2_ref[span, :]
@@ -821,32 +868,25 @@
         m1_out[span, :] = first
         m2_out[span, :] = second
         ratio_ref[low_rows(r, p), :] = ratio.astype(BF)
-        here = ratio_ref.at[low_rows(r, p)]
-        for j in (3, 1, 2):
-            send(here, here, ag_s.at[i, j - 1], ag_r.at[i, j - 1], (z, peer[j], t))
-
-    ratios(0, z)
-    w_line_rest(1)
-    w_line_rest(2)
-    for i, p in enumerate(planes):
-        arrive(zh_ref.at[share_rows(p)], zg_r.at[p])
-        ratios(1 + i, p)
-    spread(1, 1)
-    relay(1, 0)
-    spread(2, 0)
-    spread(2, 1)
-    arrive(f_ref.at[other], tp_r.at[0])
-    for n in range(2):
-        g = lax.dot_general(f_ref[n], f_ref[n], dims, preferred_element_type=F32)
-        top = g.astype(BF)
-        g_ref[n, 0] = top
-        g_ref[n, 1] = (g - top.astype(F32)).astype(BF)
-    relay(1, 1)
-    for i, p in enumerate([z] + planes):
-        for j in (1, 2, 3):
-            arrive(ratio_ref.at[low_rows(peer[j], p)], ag_r.at[i, j - 1])
-    relay(2, 0)
-    relay(2, 1)
+        ratio_in[i].start()
+
+    dims = (((0,), (0,)), ((), ()))
+
+    def low_parts():
+        for n, c_ref, span in ((0, cq_ref, slice(0, qc)), (1, cv_ref, slice(qc, cols))):
+            a = lax.dot_general(
+                low_ref[n], c_ref[...], dims, preferred_element_type=F32
+            ).astype(BF)
+            for k in range(nr):
+                part_ref[k // 2, k % 2, :, span] = a[k * own : (k + 1) * own]
+
+    def gram():
+        arrive(f_ref.at[other], tp_r.at[0])
+        for n in range(2):
+            g = lax.dot_general(f_ref[n], f_ref[n], dims, preferred_element_type=F32)
+            top = g.astype(BF)
+            g_ref[n, 0] = top
+            g_ref[n, 1] = (g - top.astype(F32)).astype(BF)
 
     def squares(n, span):
         ratio = ratio_ref[:, span]
@@ -855,20 +895,99 @@
         a = jnp.sum(a * ratio.astype(F32), axis=0, keepdims=True)
         return jnp.sum(a, axis=1, keepdims=True)
 
+    wq_in.wait()
+    wv_in.wait()
+    w_ref[at(z * rows, rows, rows), :] = wf_ref[...].astype(BF)
+    x_in.wait()
+    low_add(z, True)
+    fac_start(0)
+    w_own(0)
+    w_own(1)
+    fac_start(1)
+    fac_start(2)
+    fac[0].relay()
+    fac[1].relay()
+    w_pass(0, 0)
+    w_pass(1, 0)
+    fac[2].relay()
+    w_start(0, 0)
+    fac_finish(0)
+    w_pass(0, 1)
+    w_pass(1, 1)
+    w_start(0, 1)
+    fac_finish(1)
+    fac_finish(2)
+    low_ref[t] = acc_ref[...].astype(BF)
+    send(low_ref.at[t], low_ref.at[t], tp_s.at[1], tp_r.at[1], (z, r, other))
+    send(f_ref.at[t], f_ref.at[t], tp_s.at[0], tp_r.at[0], (z, r, other))
+    w_pass(2, 0)
+    cq_in.wait()
+    cv_in.wait()
+    arrive(low_ref.at[other], tp_r.at[1])
+    low_parts()
+    for i in range(4):
+        sum_start(i)
+    w_in[0][0].relay()
+    w_in[0][1].relay()
+    w_pass(2, 1)
+    w_own(2)
+    sum_relay(0)
+    sum_relay(1)
+    sum_relay(2)
+    sum_relay(3)
+    w_start(1, 0)
+    w_pass(0, 2)
+    w_pass(1, 2)
+    sum_finish(0)
+    sum_finish(1)
+    sum_finish(2)
+    sum_finish(3)
+    w_start(1, 1)
+    w_pass(2, 2)
+    for c in mom:
+        c.wait()
+    line_sum()
+    w_in[1][0].relay()
+    ratio_start(0)
+    w_start(2, 0)
+    ratio_start(1)
+    ratio_start(2)
+    ratio_start(3)
+    w_own(3)
+    w_in[1][1].relay()
+    w_start(2, 1)
+    ratio_in[0].relay()
+    ratio_in[1].relay()
+    ratio_in[2].relay()
+    ratio_in[3].relay()
+    w_pass(0, 3)
+    w_pass(1, 3)
+    gram()
+    w_in[2][0].relay()
+    w_pass(2, 3)
+    for i in range(4):
+        ratio_in[i].finish()
     qs = squares(0, slice(0, qc)) / (width * qc * 2)
     vs = squares(1, slice(qc, cols)) / (width * (cols - qc) * 2)
     line = lax.broadcasted_iota(jnp.int32, sq_ref.shape[1:], 0)
     sq_ref[t] = jnp.where(line == 0, qs, vs)
     send(sq_ref.at[t], sq_ref.at[t], tp_s.at[2], tp_r.at[2], (z, r, other))
+    w_in[2][1].relay()
+    for c in range(len(chunks), len(spans)):
+        for i in range(3):
+            w_land(i, c)
     arrive(sq_ref.at[other], tp_r.at[2])
     scale_out[...] = lax.rsqrt(jnp.maximum(sq_ref[0] + sq_ref[1], 0.0) + EPS_NORM)
-    for i, p in enumerate(planes):
-        arrive(w_rest(p), wz_r.at[p, len(chunks)])
+    for i in range(3):
         for c in range(len(chunks)):
-            for n, begin in ((2, 0), (3, half)):
-                arrive(w_rows(p, corner, c).at[:, pl.ds(begin, half)], wp_r.at[i, c, n])
+            w_in[i][c].finish()
     for c in sent:
         c.wait_send()
+
+    @pl.when(inner)
+    def _():
+        for c in passed:
+            c.wait_send()
 
 
 def run_line_exchange(x, cq, cv, wq, wv, qf, vf, q1, q2, v1, v2):
@@ -878,14 +997,17 @@
     rows, rank = qf.shape
     own = rank // 4
     share = own // 4
-    quarter = rows // 4 // 128 * 112
-    chunks = (quarter // 32 * 16, quarter - quarter // 32 * 16)
+    unit = rows // 64
+    quarter = 13 * unit
+    chunks = (7 * unit, 6 * unit)
+    rests = (6 * unit, 6 * unit)
     any_spec = pl.BlockSpec(memory_space=pltpu.HBM)
     vmem = pl.BlockSpec(memory_space=pltpu.VMEM)
     dma = pltpu.SemaphoreType.DMA
     n = len(chunks)
+    m = n + len(rests)
     return pl.pallas_call(
-        functools.partial(line_exchange, quarter, chunks),
+        functools.partial(line_exchange, quarter, chunks, rests),
         out_shape=(
             pltpu.VMEM((width, cols), BF),
             pltpu.VMEM((2, width, rank), BF),
@@ -903,9 +1025,12 @@
             pltpu.VMEM(cv.shape, BF),
             pltpu.VMEM((tokens, rank), F32),
             pltpu.VMEM((2, tokens, rank), BF),
-            pltpu.VMEM((rank, cols), BF),
-            pltpu.VMEM((3, own, cols), BF),
+            pltpu.VMEM((2, 2, own, cols), BF),
+            pltpu.VMEM((2, 2, own, cols // 2), BF),
+            pltpu.VMEM((2, own, cols // 2), BF),
+            pltpu.VMEM((2, own, cols // 2), BF),
             pltpu.VMEM((own, cols), BF),
+            pltpu.VMEM((share, cols), F32),
             pltpu.VMEM((4, share, cols), BF),
             pltpu.VMEM((own, cols), BF),
             pltpu.VMEM((own, cols), F32),
@@ -915,20 +1040,22 @@
             dma((10,)),
             dma((3,)),
             dma((4,)),
-            dma((3, 3)),
-            dma((3, 3)),
-            dma((3, n + 1)),
-            dma((4, n + 1)),
+            dma((3, 4)),
+            dma((3, 4)),
+            dma((5, m)),
+            dma((4, m)),
             dma((3, n, 4)),
             dma((3, n, 4)),
-            dma((4, 3)),
-            dma((4, 3)),
+            dma((4, 2)),
+            dma((4, 2)),
+            dma((4, 2)),
+            dma((4, 2)),
             dma((3,)),
             dma((4,)),
             dma((3,)),
             dma((4,)),
-            dma((4, 3)),
-            dma((4, 3)),
+            dma((4, 4)),
+            dma((4, 4)),
             dma((3,)),
             dma((3,)),
         ],

time: 91.2 us -> 75.9 us (0.83)
  the two profiles are of different devices: /device:TPU:8 before, /device:TPU:0 now
where the time goes in v2:
time: 75.9 us; the launch traced here: 75.7 us
  Pallas kernels  75.1 us (99%)
    pallas_call x1, Pallas kernels, run_line_exchange(): pl.pallas_call(functools.partial(line_exchange, quarter, chunks, rests),...  68.2 us
    pallas_call x1, Pallas kernels, run_line_finish(): pl.pallas_call(functools.partial(line_finish, steps), grid=(steps,), in_s...  6.86 us

profile of v2, /device:TPU:0, one launch (start us, length us, event | category | flops | bytes accessed | tf_op | source)
XLA Modules:
  0.0 75.7 jit_solution(10582028889963860227)
XLA Ops:
  0.6 68.2 %shard_map.186 = (bf16[2048,1536]{1,0:T(8,128)(2,1)S(1)}, bf16[2,2048,256]{2,1,0:T(8,128)(2,1)S(1)}, bf16[256,1536]{1,0:T(8,128)(2,1)S(1)}, f32[512,1536]{1,0:T(...) custom-call(bf16[768,2048]{1,0:T(8,128)(2,1)} %x_hbm.1, ...), custom_call_target="tpu_custom_call" | custom-call | tf_op jit(solution)/shard_map/pallas_call | solution.py:1009
  68.9 6.9 %shard_map.187 = (f32[512,512]{1,0:T(8,128)}, f32[512,1024]{1,0:T(8,128)}, f32[512,512]{1,0:T(8,128)}, f32[512,1024]{1,0:T(8,128)}, f32[64,512]{1,0:T(8,128)}, /...) custom-call(bf16[2048,1536]{1,0:T(8,128)(2,1)S(1)} %get-tuple-elemen, ...), custom_call_target="tpu_custom_call" | custom-call | tf_op jit(solution)/shard_map/pallas_call | solution.py:1123

commit v3 on v2

--- a/solution.py
+++ b/solution.py
@@ -555,6 +555,7 @@
     m1_out,
     m2_out,
     scale_out,
+    d_ref,
     x_ref,
     cq_ref,
     cv_ref,
@@ -573,24 +574,18 @@
     g_ref,
     sq_ref,
     local_sem,
-    fz_s,
+    out_s,
     fz_r,
-    fp_s,
     fp_r,
-    wz_s,
     wz_r,
-    wp_s,
     wp_r,
-    ra_s,
+    wc_r,
     ra_r,
-    rb_s,
     rb_r,
-    zs_s,
     zs_r,
-    zg_s,
     zg_r,
-    ag_s,
     ag_r,
+    ac_r,
     tp_s,
     tp_r,
 ):
@@ -618,7 +613,8 @@
     far = 3 - 3 * upper
     planes = [near, mid, far]
     inner = jnp.logical_and(z > 0, z < nz - 1)
-    sent, passed = [], []
+    groups = {"plane": 0, "line": 1, "inner": 2}
+    sent = dict.fromkeys(groups, 0)
 
     def remote(src, dst, ss, rs, dev):
         return pltpu.make_async_remote_copy(
@@ -630,18 +626,32 @@
             device_id_type=pl.DeviceIdType.MESH,
         )
 
-    def send(src, dst, ss, rs, dev):
-        c = remote(src, dst, ss, rs, dev)
-        c.start()
-        sent.append(c)
-
-    def send_inner(src, dst, ss, rs, dev):
-        c = remote(src, dst, ss, rs, dev)
-        passed.append(c)
+    def count(ref, group):
+        sent[group] += ref.size * ref.dtype.itemsize
+
+    def send(src, dst, rs, dev, group="plane"):
+        count(dst, group)
+        remote(src, dst, out_s.at[groups[group]], rs, dev).start()
+
+    def send_pair(src, dst, n):
+        remote(src, dst, tp_s.at[n], tp_r.at[n], (z, r, other)).start()
+
+    def send_inner(ref, rs, dev, wait=None):
+        count(ref, "inner")
 
         @pl.when(inner)
         def _():
-            c.start()
+            if wait is not None:
+                arrive(ref, wait)
+            remote(ref, ref, out_s.at[2], rs, dev).start()
+
+    def drain(group):
+        size, line = sent[group], cols * 2
+        while size:
+            span = pl.ds(0, min(size // line, width))
+            size -= min(size // line, width) * line
+            ref = w_ref.at[span]
+            remote(ref, ref, out_s.at[groups[group]], tp_r.at[0], (z, r, other)).wait_send()
 
     def arrive(dst, rs):
         remote(dst, dst, tp_s.at[0], rs, (z, r, other)).wait_recv()
@@ -661,24 +671,23 @@
         fac_copy(vf_hbm).start()
 
     left, right = pl.ds(0, qc), pl.ds(qc, cols - qc)
-    wq_in = pltpu.make_async_copy(wq_hbm, wf_ref.at[:, left], local_sem.at[1])
-    wv_in = pltpu.make_async_copy(wv_hbm, wf_ref.at[:, right], local_sem.at[2])
-    x_in = pltpu.make_async_copy(x_hbm, x_ref, local_sem.at[3])
-    cq_in = pltpu.make_async_copy(cq_hbm, cq_ref, local_sem.at[4])
-    cv_in = pltpu.make_async_copy(cv_hbm, cv_ref, local_sem.at[5])
-    mom = [
-        pltpu.make_async_copy(src, dst.at[:, span], local_sem.at[6 + n])
-        for n, (src, dst, span) in enumerate(
-            (
-                (q1_hbm, m1_ref, left),
-                (v1_hbm, m1_ref, right),
-                (q2_hbm, m2_ref, left),
-                (v2_hbm, m2_ref, right),
-            )
-        )
-    ]
-    for c in [wq_in, wv_in, x_in, cq_in, cv_in] + mom:
+    x_in = pltpu.make_async_copy(x_hbm, x_ref, local_sem.at[1])
+    cq_in = pltpu.make_async_copy(cq_hbm, cq_ref, local_sem.at[2])
+    cv_in = pltpu.make_async_copy(cv_hbm, cv_ref, local_sem.at[3])
+    pltpu.make_async_copy(wq_hbm, wf_ref.at[:, left], local_sem.at[4]).start()
+    pltpu.make_async_copy(wv_hbm, wf_ref.at[:, right], local_sem.at[4]).start()
+    for c in (x_in, cq_in, cv_in):
         c.start()
+    for n, src, dst, span in (
+        (5, q1_hbm, m1_ref, left),
+        (5, v1_hbm, m1_ref, right),
+        (6, q2_hbm, m2_ref, left),
+        (6, v2_hbm, m2_ref, right),
+    ):
+        pltpu.make_async_copy(src, dst.at[:, span], local_sem.at[n]).start()
+
+    def loaded(ref, n):
+        pltpu.make_async_copy(ref, ref, local_sem.at[n]).wait()
 
     barrier = pltpu.get_barrier_semaphore()
     peers = [(p, r, t) for p in planes]
@@ -691,24 +700,20 @@
     pl.semaphore_wait(barrier, len(peers))
 
     class Spread:
-        def __init__(self, view, split, ss, rs):
-            self.view, self.split, self.ss, self.rs = view, split, ss, rs
+        def __init__(self, view, split, rs, rest):
+            self.view, self.split, self.rs, self.rest = view, split, rs, rest
 
         def start(self):
             here = self.view(r)
             for n, dev in ((0, side), (1, over)):
-                send(here, here, self.ss.at[n], self.rs.at[n], (z, dev, t))
+                send(here, here, self.rs.at[n], (z, dev, t))
 
         def relay(self):
             for n, src, dev in ((0, side, over), (1, over, side)):
                 whole = self.view(src)
                 arrive(whole, self.rs.at[n])
                 there = self.split(whole, n)
-                send(there, there, self.ss.at[2 + n], self.rs.at[2 + n], (z, dev, t))
-
-        def finish(self):
-            for n in range(2):
-                arrive(self.split(self.view(corner), n), self.rs.at[2 + n])
+                send(there, there, self.rest, (z, dev, t))
 
     def halves(ref, n):
         return ref.at[:, pl.ds(n * half, half)]
@@ -719,7 +724,7 @@
     fac_copy(qf_hbm).wait()
     for i, p in enumerate(planes):
         here = fac_rows(z, r)
-        send(here, here, fz_s.at[i], fz_r.at[z], (p, r, t))
+        send(here, here, fz_r.at[z], (p, r, t), "line")
 
     spans = [(n, s, True) for n, s in zip([sum(chunks[:c]) for c in range(len(chunks))], chunks)]
     spans += [(n, s, False) for n, s in zip([sum(rests[:c]) for c in range(len(rests))], rests)]
@@ -731,19 +736,12 @@
 
     def w_own(c):
         here = w_rows(z, r, c)
-        send(here, here, wz_s.at[3, c], wz_r.at[z, c], (near, r, t))
-        send_inner(here, here, wz_s.at[4, c], wz_r.at[z, c], (mid, r, t))
+        send(here, here, wz_r.at[z, c], (near, r, t), "line")
+        send_inner(here, wz_r.at[z, c], (mid, r, t))
 
     def w_pass(i, c):
-        here = w_rows(planes[i], r, c)
-        to = near if i else mid
-        copy = remote(here, here, wz_s.at[i, c], wz_r.at[planes[i], c], (to, r, t))
-        passed.append(copy)
-
-        @pl.when(inner)
-        def _():
-            arrive(here, wz_r.at[planes[i], c])
-            copy.start()
+        sem = wz_r.at[planes[i], c]
+        send_inner(w_rows(planes[i], r, c), sem, (near if i else mid, r, t), sem)
 
     def w_land(i, c):
         @pl.when(jnp.logical_not(inner))
@@ -756,7 +754,7 @@
 
     w_in = [
         [
-            Spread(functools.partial(lambda p, c, rr: w_rows(p, rr, c), p, c), halves, wp_s.at[i, c], wp_r.at[i, c])
+            Spread(functools.partial(lambda p, c, rr: w_rows(p, rr, c), p, c), halves, wp_r.at[i, c], wc_r.at[i])
             for c in range(len(chunks))
         ]
         for i, p in enumerate(planes)
@@ -779,8 +777,8 @@
         Spread(
             functools.partial(fac_rows, p),
             lambda ref, n: ref.at[pl.ds(n * (part // 2), part // 2)],
-            fp_s.at[i],
             fp_r.at[i],
+            fp_r.at[i, 2],
         )
         for i, p in enumerate(planes)
     ]
@@ -790,7 +788,7 @@
         fac[i].start()
 
     def fac_finish(i):
-        fac[i].finish()
+        arrive(fac_rows(planes[i], corner), fp_r.at[i, 2])
         low_add(planes[i], False)
 
     def share_rows(plane):
@@ -808,7 +806,7 @@
             (0, part_ref.at[:, 1 - px, span, lo], side),
             (1, part_ref.at[1 - py, :, span, hi], over),
         ):
-            send(src, ra_ref.at[n, :, span], ra_s.at[i, n], ra_r.at[i, n], (z, dev, t))
+            send(src, ra_ref.at[n, :, span], ra_r.at[i, n], (z, dev, t))
 
     def sum_relay(i):
         span = share_rows(order[i])
@@ -819,7 +817,7 @@
             (1, part_ref[py, 1 - px, span, hi], ra_ref[1, 1 - px, span, :], side),
         ):
             tb_ref[n, span, :] = (mine.astype(F32) + theirs.astype(F32)).astype(BF)
-            send(tb_ref.at[n, span], rb_ref.at[n, span], rb_s.at[i, n], rb_r.at[i, n], (z, dev, t))
+            send(tb_ref.at[n, span], rb_ref.at[n, span], rb_r.at[i, n], (z, dev, t))
 
     def sum_finish(i):
         span = share_rows(order[i])
@@ -834,7 +832,7 @@
         else:
             zs_ref[span, lo] = out[0].astype(BF)
             zs_ref[span, hi] = out[1].astype(BF)
-            send(zs_ref.at[span], z_ref.at[z], zs_s.at[i], zs_r.at[z], (order[i], r, t))
+            send(zs_ref.at[span], z_ref.at[z], zs_r.at[z], (order[i], r, t), "line")
 
     def line_sum():
         proj = zo_ref[...]
@@ -843,15 +841,15 @@
             proj = proj + z_ref[p].astype(F32)
         here = zh_ref.at[share_rows(z)]
         zh_ref[share_rows(z), :] = proj.astype(BF)
-        for i, p in ((2, far), (1, mid), (0, near)):
-            send(here, here, zg_s.at[i], zg_r.at[z], (p, r, t))
+        for p in (far, mid, near):
+            send(here, here, zg_r.at[z], (p, r, t), "line")
 
     ratio_in = [
         Spread(
             functools.partial(lambda p, rr: ratio_ref.at[low_rows(rr, p)], p),
             halves,
-            ag_s.at[i],
             ag_r.at[i],
+            ac_r.at[0],
         )
         for i, p in enumerate([z] + planes)
     ]
@@ -895,8 +893,20 @@
         a = jnp.sum(a * ratio.astype(F32), axis=0, keepdims=True)
         return jnp.sum(a, axis=1, keepdims=True)
 
-    wq_in.wait()
-    wv_in.wait()
+    def own_rows():
+        tile = rows // 8
+
+        @pl.loop(0, 8)
+        def _(i):
+            mine = at(z * rows + i * tile, tile, tile)
+            span = at(i * tile, tile, tile)
+            for n, cut in ((0, slice(0, qc)), (1, slice(qc, cols))):
+                d = jnp.dot(f_ref[n, mine], ratio_ref[:, cut], preferred_element_type=F32)
+                d = d * scale_out[n : n + 1, 0:1]
+                d_ref[span, cut] = d
+                wf_ref[span, cut] = wf_ref[span, cut] - RATE * d
+
+    loaded(wf_ref, 4)
     w_ref[at(z * rows, rows, rows), :] = wf_ref[...].astype(BF)
     x_in.wait()
     low_add(z, True)
@@ -918,8 +928,8 @@
     fac_finish(1)
     fac_finish(2)
     low_ref[t] = acc_ref[...].astype(BF)
-    send(low_ref.at[t], low_ref.at[t], tp_s.at[1], tp_r.at[1], (z, r, other))
-    send(f_ref.at[t], f_ref.at[t], tp_s.at[0], tp_r.at[0], (z, r, other))
+    send_pair(low_ref.at[t], low_ref.at[t], 1)
+    send_pair(f_ref.at[t], f_ref.at[t], 0)
     w_pass(2, 0)
     cq_in.wait()
     cv_in.wait()
@@ -944,8 +954,8 @@
     sum_finish(3)
     w_start(1, 1)
     w_pass(2, 2)
-    for c in mom:
-        c.wait()
+    loaded(m1_ref, 5)
+    loaded(m2_ref, 6)
     line_sum()
     w_in[1][0].relay()
     ratio_start(0)
@@ -965,29 +975,29 @@
     gram()
     w_in[2][0].relay()
     w_pass(2, 3)
-    for i in range(4):
-        ratio_in[i].finish()
+    arrive(ratio_ref.at[at(corner * own, own, own)], ac_r.at[0])
     qs = squares(0, slice(0, qc)) / (width * qc * 2)
     vs = squares(1, slice(qc, cols)) / (width * (cols - qc) * 2)
     line = lax.broadcasted_iota(jnp.int32, sq_ref.shape[1:], 0)
     sq_ref[t] = jnp.where(line == 0, qs, vs)
-    send(sq_ref.at[t], sq_ref.at[t], tp_s.at[2], tp_r.at[2], (z, r, other))
+    send_pair(sq_ref.at[t], sq_ref.at[t], 2)
     w_in[2][1].relay()
+    arrive(sq_ref.at[other], tp_r.at[2])
+    scale_out[...] = lax.rsqrt(jnp.maximum(sq_ref[0] + sq_ref[1], 0.0) + EPS_NORM)
+    own_rows()
     for c in range(len(chunks), len(spans)):
         for i in range(3):
             w_land(i, c)
-    arrive(sq_ref.at[other], tp_r.at[2])
-    scale_out[...] = lax.rsqrt(jnp.maximum(sq_ref[0] + sq_ref[1], 0.0) + EPS_NORM)
     for i in range(3):
-        for c in range(len(chunks)):
-            w_in[i][c].finish()
-    for c in sent:
-        c.wait_send()
+        arrive(w_ref.at[at(planes[i] * rows + corner * quarter, quarter, 8)], wc_r.at[i])
+    for n, ref in enumerate((f_ref.at[t], low_ref.at[t], sq_ref.at[t])):
+        remote(ref, ref, tp_s.at[n], tp_r.at[n], (z, r, other)).wait_send()
+    drain("plane")
+    drain("line")
 
     @pl.when(inner)
     def _():
-        for c in passed:
-            c.wait_send()
+        drain("inner")
 
 
 def run_line_exchange(x, cq, cv, wq, wv, qf, vf, q1, q2, v1, v2):
@@ -1016,9 +1026,10 @@
             pltpu.VMEM((own, cols), F32),
             pltpu.VMEM((own, cols), F32),
             pltpu.VMEM((8, 128), F32),
+            pltpu.VMEM((rows, cols), F32),
         ),
         in_specs=[any_spec] * 11,
-        out_specs=(vmem,) * 7,
+        out_specs=(vmem,) * 8,
         scratch_shapes=[
             pltpu.VMEM((tokens, width), BF),
             pltpu.VMEM(cq.shape, BF),
@@ -1037,25 +1048,19 @@
             pltpu.VMEM((own, cols), F32),
             pltpu.VMEM((2, 2, rank, rank), BF),
             pltpu.VMEM((2, 8, 128), F32),
-            dma((10,)),
+            dma((7,)),
             dma((3,)),
             dma((4,)),
-            dma((3, 4)),
-            dma((3, 4)),
-            dma((5, m)),
+            dma((3, 3)),
             dma((4, m)),
-            dma((3, n, 4)),
-            dma((3, n, 4)),
+            dma((3, n, 2)),
+            dma((3,)),
             dma((4, 2)),
             dma((4, 2)),
+            dma((4,)),
+            dma((4,)),
             dma((4, 2)),
-            dma((4, 2)),
-            dma((3,)),
-            dma((4,)),
-            dma((3,)),
-            dma((4,)),
-            dma((4, 4)),
-            dma((4, 4)),
+            dma((1,)),
             dma((3,)),
             dma((3,)),
         ],
@@ -1070,10 +1075,11 @@
     w_ref,
     f_ref,
     ratio_ref,
-    wf_ref,
+    m_ref,
     m1_ref,
     m2_ref,
     scale_ref,
+    d_ref,
     qd_out,
     vd_out,
     qm_out,
@@ -1084,58 +1090,55 @@
     v2_out,
     qcopy_out,
     vcopy_out,
+    c_ref,
+    sem,
 ):
-    i = pl.program_id(0)
-    z = lax.axis_index("fs")
-    rows, cols = wf_ref.shape
+    width, cols = w_ref.shape
     qc = qd_out.shape[1]
-    tall, small, low = w_ref.shape[0] // steps, rows // steps, m1_ref.shape[0] // steps
-    every = pl.ds(pl.multiple_of(i * tall, tall), tall)
-    mine = pl.ds(pl.multiple_of(z * rows + i * small, small), small)
-    here = pl.ds(pl.multiple_of(i * small, small), small)
-    moment = pl.ds(pl.multiple_of(i * low, low), low)
-    sets = (
-        (0, slice(0, qc), qd_out, qm_out, q1_out, q2_out, qcopy_out),
-        (1, slice(qc, cols), vd_out, vm_out, v1_out, v2_out, vcopy_out),
+    left, right = pl.ds(0, qc), pl.ds(qc, cols - qc)
+    outs = (
+        (d_ref, left, qd_out),
+        (d_ref, right, vd_out),
+        (m_ref, left, qm_out),
+        (m_ref, right, vm_out),
+        (m1_ref, left, q1_out),
+        (m1_ref, right, v1_out),
+        (m2_ref, left, q2_out),
+        (m2_ref, right, v2_out),
     )
-    for n, at, d_out, m_out, m1_out, m2_out, c_out in sets:
-        scale = scale_ref[n : n + 1, 0:1]
-        ratio = ratio_ref[:, at]
-        d = jnp.dot(f_ref[n, mine], ratio, preferred_element_type=F32) * scale
-        d_out[...] = d
-        m_out[...] = wf_ref[here, at] - RATE * d
-        m1_out[...] = m1_ref[moment, at]
-        m2_out[...] = m2_ref[moment, at]
-        raw = jnp.dot(f_ref[n, every], ratio, preferred_element_type=F32)
-        c_out[...] = (w_ref[every, at].astype(F32) - RATE * (raw * scale)).astype(BF)
-
-
-def run_line_finish(weights, factors, ratio, wf, m1, m2, scale, qc):
-    rows, cols = wf.shape
+    copies = [
+        pltpu.make_async_copy(src.at[:, cut], dst, sem.at[n])
+        for n, (src, cut, dst) in enumerate(outs)
+    ]
+    for c in copies:
+        c.start()
+    tall = width // steps
+
+    @pl.loop(0, steps)
+    def _(i):
+        span = pl.ds(pl.multiple_of(i * tall, tall), tall)
+        for n, cut, dst in ((0, left, qcopy_out), (1, right, vcopy_out)):
+            raw = jnp.dot(f_ref[n, span], ratio_ref[:, cut], preferred_element_type=F32)
+            raw = raw * scale_ref[n : n + 1, 0:1]
+            c_ref[span, cut] = (w_ref[span, cut].astype(F32) - RATE * raw).astype(BF)
+            pltpu.make_async_copy(c_ref.at[span, cut], dst.at[span], sem.at[8 + n]).start()
+
+    for c in copies:
+        c.wait()
+    for n, cut, dst in ((0, left, qcopy_out), (1, right, vcopy_out)):
+        pltpu.make_async_copy(c_ref.at[:, cut], dst, sem.at[8 + n]).wait()
+
+
+def run_line_finish(weights, factors, ratio, masters, m1, m2, scale, directions, qc):
+    rows, cols = masters.shape
     vc = cols - qc
     width, own = weights.shape[0], m1.shape[0]
-    steps = 8
-
-    def tall(n, c):
-        return pl.BlockSpec((n // steps, c), lambda i: (i, 0))
-
+    vmem = pl.BlockSpec(memory_space=pltpu.VMEM)
     shape = jax.ShapeDtypeStruct
     return pl.pallas_call(
-        functools.partial(line_finish, steps),
-        grid=(steps,),
-        in_specs=[pl.BlockSpec(memory_space=pltpu.VMEM)] * 7,
-        out_specs=[
-            tall(rows, qc),
-            tall(rows, vc),
-            tall(rows, qc),
-            tall(rows, vc),
-            tall(own, qc),
-            tall(own, qc),
-            tall(own, vc),
-            tall(own, vc),
-            tall(width, qc),
-            tall(width, vc),
-        ],
+        functools.partial(line_finish, 8),
+        in_specs=[vmem] * 8,
+        out_specs=[pl.BlockSpec(memory_space=pltpu.HBM)] * 10,
         out_shape=[
             shape((rows, qc), F32),
             shape((rows, vc), F32),
@@ -1148,8 +1151,9 @@
             shape((width, qc), BF),
             shape((width, vc), BF),
         ],
-        compiler_params=pltpu.CompilerParams(vmem_limit_bytes=24 * 1024 * 1024),
-    )(weights, factors, ratio, wf, m1, m2, scale)
+        scratch_shapes=[pltpu.VMEM((width, cols), BF), pltpu.SemaphoreType.DMA((10,))],
+        compiler_params=pltpu.CompilerParams(vmem_limit_bytes=16 * 1024 * 1024),
+    )(weights, factors, ratio, masters, m1, m2, scale, directions)
 
 
 def suits_line(nz, nr, qf, cq, cv):

time: 75.9 us -> 72.7 us (0.958)
  Pallas kernels: 75.1 us -> 71.9 us
    pallas_call x1, Pallas kernels: 6.86 us -> 4.86 us  [run_line_finish(): pl.pallas_call(functools.partial(line_finish, 8), in_specs=[vmem] * 8, ou...]
    pallas_call x1, Pallas kernels: 68.2 us -> 67 us  [run_line_exchange(): pl.pallas_call(functools.partial(line_exchange, quarter, chunks, rests),...]
where the time goes in v3:
time: 72.7 us; the launch traced here: 72.6 us
  Pallas kernels  71.9 us (99%)
    pallas_call x1, Pallas kernels, run_line_exchange(): pl.pallas_call(functools.partial(line_exchange, quarter, chunks, rests),...  67 us
    pallas_call x1, Pallas kernels, run_line_finish(): pl.pallas_call(functools.partial(line_finish, 8), in_specs=[vmem] * 8, ou...  4.86 us

profile of v3, /device:TPU:0, one launch (start us, length us, event | category | flops | bytes accessed | tf_op | source)
XLA Modules:
  0.0 72.6 jit_solution(7794198818243781171)
XLA Ops:
  0.6 67.0 %shard_map.186 = (bf16[2048,1536]{1,0:T(8,128)(2,1)S(1)}, bf16[2,2048,256]{2,1,0:T(8,128)(2,1)S(1)}, bf16[256,1536]{1,0:T(8,128)(2,1)S(1)}, f32[512,1536]{1,0:T(...) custom-call(bf16[768,2048]{1,0:T(8,128)(2,1)} %x_hbm.1, ...), custom_call_target="tpu_custom_call" | custom-call | tf_op jit(solution)/shard_map/pallas_call | solution.py:1019
  67.7 4.9 %shard_map.187 = (f32[512,512]{1,0:T(8,128)}, f32[512,1024]{1,0:T(8,128)}, f32[512,512]{1,0:T(8,128)}, f32[512,1024]{1,0:T(8,128)}, f32[64,512]{1,0:T(8,128)}, /...) custom-call(bf16[2048,1536]{1,0:T(8,128)(2,1)S(1)} %get-tuple-elemen, ...), custom_call_target="tpu_custom_call" | custom-call | tf_op jit(solution)/shard_map/pallas_call | solution.py:1138

commit v4 on v3

--- a/solution.py
+++ b/solution.py
@@ -761,17 +761,12 @@
     ]
 
     def low_add(plane, first):
-        tile = tokens // 3
-
-        @pl.loop(0, 3)
-        def _(n):
-            span = at(n * tile, tile, 16)
-            a = jnp.dot(
-                x_ref[span, at(plane * rows, rows, rows)],
-                f_ref[t, at(plane * rows, rows, rows)],
-                preferred_element_type=F32,
-            )
-            acc_ref[span, :] = a if first else acc_ref[span, :] + a
+        a = jnp.dot(
+            x_ref[:, at(plane * rows, rows, rows)],
+            f_ref[t, at(plane * rows, rows, rows)],
+            preferred_element_type=F32,
+        )
+        acc_ref[...] = a if first else acc_ref[...] + a
 
     fac = [
         Spread(
@@ -894,94 +889,111 @@
         return jnp.sum(a, axis=1, keepdims=True)
 
     def own_rows():
-        tile = rows // 8
-
-        @pl.loop(0, 8)
-        def _(i):
-            mine = at(z * rows + i * tile, tile, tile)
-            span = at(i * tile, tile, tile)
-            for n, cut in ((0, slice(0, qc)), (1, slice(qc, cols))):
-                d = jnp.dot(f_ref[n, mine], ratio_ref[:, cut], preferred_element_type=F32)
-                d = d * scale_out[n : n + 1, 0:1]
-                d_ref[span, cut] = d
-                wf_ref[span, cut] = wf_ref[span, cut] - RATE * d
+        mine = at(z * rows, rows, rows)
+        tile = min(256, qc)
+
+        def columns(n, begin):
+            cut = pl.ds(begin, tile)
+            d = jnp.dot(f_ref[n, mine], ratio_ref[:, cut], preferred_element_type=F32)
+            d = d * scale_out[n : n + 1, 0:1]
+            d_ref[:, cut] = d
+            wf_ref[:, cut] = wf_ref[:, cut] - RATE * d
+
+        for begin in range(0, cols, tile):
+            columns(0 if begin < qc else 1, begin)
 
     loaded(wf_ref, 4)
     w_ref[at(z * rows, rows, rows), :] = wf_ref[...].astype(BF)
+    w_own(2)
+    fac_start(0)
+    w_own(1)
     x_in.wait()
     low_add(z, True)
-    fac_start(0)
-    w_own(0)
-    w_own(1)
     fac_start(1)
     fac_start(2)
+    w_own(0)
     fac[0].relay()
     fac[1].relay()
-    w_pass(0, 0)
-    w_pass(1, 0)
+    w_own(4)
+    w_pass(1, 2)
+    w_pass(0, 2)
     fac[2].relay()
-    w_start(0, 0)
+    w_start(0, 2)
+    w_own(3)
     fac_finish(0)
     w_pass(0, 1)
-    w_pass(1, 1)
+    fac_finish(1)
     w_start(0, 1)
-    fac_finish(1)
     fac_finish(2)
+    send_pair(f_ref.at[t], f_ref.at[t], 0)
+    w_own(5)
     low_ref[t] = acc_ref[...].astype(BF)
     send_pair(low_ref.at[t], low_ref.at[t], 1)
-    send_pair(f_ref.at[t], f_ref.at[t], 0)
-    w_pass(2, 0)
+    w_pass(0, 0)
+    w_start(1, 2)
     cq_in.wait()
     cv_in.wait()
     arrive(low_ref.at[other], tp_r.at[1])
     low_parts()
-    for i in range(4):
-        sum_start(i)
+    sum_start(2)
+    sum_start(0)
+    w_pass(1, 0)
+    sum_start(1)
+    w_pass(1, 1)
+    sum_start(3)
+    sum_relay(2)
+    sum_relay(0)
+    w_pass(0, 5)
+    w_start(0, 0)
+    w_pass(2, 1)
+    sum_relay(3)
+    sum_relay(1)
+    w_in[1][2].relay()
+    sum_finish(2)
+    w_in[0][1].relay()
+    w_pass(1, 5)
+    sum_finish(0)
+    w_start(1, 0)
+    gram()
+    w_pass(2, 0)
+    sum_finish(3)
     w_in[0][0].relay()
-    w_in[0][1].relay()
-    w_pass(2, 1)
-    w_own(2)
-    sum_relay(0)
-    sum_relay(1)
-    sum_relay(2)
-    sum_relay(3)
-    w_start(1, 0)
-    w_pass(0, 2)
-    w_pass(1, 2)
-    sum_finish(0)
+    w_start(2, 1)
     sum_finish(1)
-    sum_finish(2)
-    sum_finish(3)
     w_start(1, 1)
-    w_pass(2, 2)
     loaded(m1_ref, 5)
     loaded(m2_ref, 6)
     line_sum()
+    ratio_start(0)
+    w_pass(0, 4)
+    w_pass(2, 5)
+    w_pass(2, 2)
     w_in[1][0].relay()
-    ratio_start(0)
+    w_pass(1, 3)
     w_start(2, 0)
+    ratio_in[0].relay()
+    w_pass(0, 3)
+    ratio_start(3)
     ratio_start(1)
     ratio_start(2)
-    ratio_start(3)
-    w_own(3)
-    w_in[1][1].relay()
-    w_start(2, 1)
-    ratio_in[0].relay()
+    w_in[2][1].relay()
+    w_start(2, 2)
+    w_pass(2, 4)
+    w_pass(1, 4)
+    w_pass(2, 3)
     ratio_in[1].relay()
     ratio_in[2].relay()
     ratio_in[3].relay()
-    w_pass(0, 3)
-    w_pass(1, 3)
-    gram()
+    w_in[0][2].relay()
+    w_in[2][2].relay()
     w_in[2][0].relay()
-    w_pass(2, 3)
+    w_in[1][1].relay()
     arrive(ratio_ref.at[at(corner * own, own, own)], ac_r.at[0])
     qs = squares(0, slice(0, qc)) / (width * qc * 2)
     vs = squares(1, slice(qc, cols)) / (width * (cols - qc) * 2)
     line = lax.broadcasted_iota(jnp.int32, sq_ref.shape[1:], 0)
     sq_ref[t] = jnp.where(line == 0, qs, vs)
     send_pair(sq_ref.at[t], sq_ref.at[t], 2)
-    w_in[2][1].relay()
     arrive(sq_ref.at[other], tp_r.at[2])
     scale_out[...] = lax.rsqrt(jnp.maximum(sq_ref[0] + sq_ref[1], 0.0) + EPS_NORM)
     own_rows()
@@ -1008,9 +1020,9 @@
     own = rank // 4
     share = own // 4
     unit = rows // 64
-    quarter = 13 * unit
-    chunks = (7 * unit, 6 * unit)
-    rests = (6 * unit, 6 * unit)
+    quarter = 12 * unit
+    chunks = (4 * unit, 4 * unit, 4 * unit)
+    rests = (6 * unit, 5 * unit, 5 * unit)
     any_spec = pl.BlockSpec(memory_space=pltpu.HBM)
     vmem = pl.BlockSpec(memory_space=pltpu.VMEM)
     dma = pltpu.SemaphoreType.DMA

time: 72.7 us -> 68 us (0.935)
  Pallas kernels: 71.9 us -> 67.1 us
    pallas_call x1, Pallas kernels: 67 us -> 62.3 us  [run_line_exchange(): pl.pallas_call(functools.partial(line_exchange, quarter, chunks, rests),...]
where the time goes in v4:
time: 68 us; the launch traced here: 67.8 us
  Pallas kernels  67.1 us (99%)
    pallas_call x1, Pallas kernels, run_line_exchange(): pl.pallas_call(functools.partial(line_exchange, quarter, chunks, rests),...  62.3 us
    pallas_call x1, Pallas kernels, run_line_finish(): pl.pallas_call(functools.partial(line_finish, 8), in_specs=[vmem] * 8, ou...  4.86 us

profile of v4, /device:TPU:0, one launch (start us, length us, event | category | flops | bytes accessed | tf_op | source)
XLA Modules:
  0.0 67.8 jit_solution(16801671628199594669)
XLA Ops:
  0.6 62.3 %shard_map.186 = (bf16[2048,1536]{1,0:T(8,128)(2,1)S(1)}, bf16[2,2048,256]{2,1,0:T(8,128)(2,1)S(1)}, bf16[256,1536]{1,0:T(8,128)(2,1)S(1)}, f32[512,1536]{1,0:T(...) custom-call(bf16[768,2048]{1,0:T(8,128)(2,1)} %x_hbm.1, ...), custom_call_target="tpu_custom_call" | custom-call | tf_op jit(solution)/shard_map/pallas_call | solution.py:1031
  62.9 4.9 %shard_map.187 = (f32[512,512]{1,0:T(8,128)}, f32[512,1024]{1,0:T(8,128)}, f32[512,512]{1,0:T(8,128)}, f32[512,1024]{1,0:T(8,128)}, f32[64,512]{1,0:T(8,128)}, /...) custom-call(bf16[2048,1536]{1,0:T(8,128)(2,1)S(1)} %get-tuple-elemen, ...), custom_call_target="tpu_custom_call" | custom-call | tf_op jit(solution)/shard_map/pallas_call | solution.py:1150

commit v5 on v4

--- a/solution.py
+++ b/solution.py
@@ -700,19 +700,18 @@
     pl.semaphore_wait(barrier, len(peers))
 
     class Spread:
-        def __init__(self, view, split, rs, rest):
-            self.view, self.split, self.rs, self.rest = view, split, rs, rest
+        def __init__(self, view, split, both, rs, rest):
+            self.view, self.split, self.both, self.rs, self.rest = view, split, both, rs, rest
 
         def start(self):
             here = self.view(r)
-            for n, dev in ((0, side), (1, over)):
-                send(here, here, self.rs.at[n], (z, dev, t))
+            for dev in (side, over):
+                send(here, here, self.rs, (z, dev, t))
 
         def relay(self):
+            arrive(self.both, self.rs)
             for n, src, dev in ((0, side, over), (1, over, side)):
-                whole = self.view(src)
-                arrive(whole, self.rs.at[n])
-                there = self.split(whole, n)
+                there = self.split(self.view(src), n)
                 send(there, there, self.rest, (z, dev, t))
 
     def halves(ref, n):
@@ -736,17 +735,17 @@
 
     def w_own(c):
         here = w_rows(z, r, c)
-        send(here, here, wz_r.at[z, c], (near, r, t), "line")
-        send_inner(here, wz_r.at[z, c], (mid, r, t))
+        send(here, here, wz_r.at[0, c], (near, r, t), "line")
+        send_inner(here, wz_r.at[1, c], (mid, r, t))
 
     def w_pass(i, c):
-        sem = wz_r.at[planes[i], c]
-        send_inner(w_rows(planes[i], r, c), sem, (near if i else mid, r, t), sem)
+        to, sem = (near, wz_r.at[i, c]) if i else (mid, wz_r.at[2, c])
+        send_inner(w_rows(planes[i], r, c), sem, (to, r, t), wz_r.at[i, c])
 
     def w_land(i, c):
         @pl.when(jnp.logical_not(inner))
         def _():
-            arrive(w_rows(planes[i], r, c), wz_r.at[planes[i], c])
+            arrive(w_rows(planes[i], r, c), wz_r.at[i, c])
 
     def w_start(i, c):
         w_land(i, c)
@@ -754,7 +753,7 @@
 
     w_in = [
         [
-            Spread(functools.partial(lambda p, c, rr: w_rows(p, rr, c), p, c), halves, wp_r.at[i, c], wc_r.at[i])
+            Spread(functools.partial(lambda p, c, rr: w_rows(p, rr, c), p, c), halves, w_ref.at[pl.ds(0, 2 * chunks[c])], wp_r.at[i, c], wc_r.at[i])
             for c in range(len(chunks))
         ]
         for i, p in enumerate(planes)
@@ -772,8 +771,9 @@
         Spread(
             functools.partial(fac_rows, p),
             lambda ref, n: ref.at[pl.ds(n * (part // 2), part // 2)],
-            fp_r.at[i],
-            fp_r.at[i, 2],
+            f_ref.at[t, pl.ds(0, 2 * part)],
+            fp_r.at[i, 0],
+            fp_r.at[i, 1],
         )
         for i, p in enumerate(planes)
     ]
@@ -783,7 +783,7 @@
         fac[i].start()
 
     def fac_finish(i):
-        arrive(fac_rows(planes[i], corner), fp_r.at[i, 2])
+        arrive(fac_rows(planes[i], corner), fp_r.at[i, 1])
         low_add(planes[i], False)
 
     def share_rows(plane):
@@ -801,23 +801,21 @@
             (0, part_ref.at[:, 1 - px, span, lo], side),
             (1, part_ref.at[1 - py, :, span, hi], over),
         ):
-            send(src, ra_ref.at[n, :, span], ra_r.at[i, n], (z, dev, t))
+            send(src, ra_ref.at[n, :, span], ra_r.at[i], (z, dev, t))
 
     def sum_relay(i):
         span = share_rows(order[i])
-        for n in range(2):
-            arrive(ra_ref.at[n, :, span], ra_r.at[i, n])
+        arrive(ra_ref.at[:, :, span], ra_r.at[i])
         for n, mine, theirs, dev in (
             (0, part_ref[1 - py, px, span, lo], ra_ref[0, 1 - py, span, :], over),
             (1, part_ref[py, 1 - px, span, hi], ra_ref[1, 1 - px, span, :], side),
         ):
             tb_ref[n, span, :] = (mine.astype(F32) + theirs.astype(F32)).astype(BF)
-            send(tb_ref.at[n, span], rb_ref.at[n, span], rb_r.at[i, n], (z, dev, t))
+            send(tb_ref.at[n, span], rb_ref.at[n, span], rb_r.at[i], (z, dev, t))
 
     def sum_finish(i):
         span = share_rows(order[i])
-        for n in range(2):
-            arrive(rb_ref.at[n, span], rb_r.at[i, n])
+        arrive(rb_ref.at[:, span], rb_r.at[i])
         out = []
         for n, cut, theirs in ((0, lo, ra_ref[0, py, span, :]), (1, hi, ra_ref[1, px, span, :])):
             a = part_ref[py, px, span, cut].astype(F32) + theirs.astype(F32)
@@ -843,6 +841,7 @@
         Spread(
             functools.partial(lambda p, rr: ratio_ref.at[low_rows(rr, p)], p),
             halves,
+            ratio_ref.at[pl.ds(0, 2 * share)],
             ag_r.at[i],
             ac_r.at[0],
         )
@@ -913,9 +912,9 @@
     fac_start(2)
     w_own(0)
     fac[0].relay()
+    w_pass(1, 2)
     fac[1].relay()
     w_own(4)
-    w_pass(1, 2)
     w_pass(0, 2)
     fac[2].relay()
     w_start(0, 2)
@@ -926,9 +925,9 @@
     w_start(0, 1)
     fac_finish(2)
     send_pair(f_ref.at[t], f_ref.at[t], 0)
-    w_own(5)
     low_ref[t] = acc_ref[...].astype(BF)
     send_pair(low_ref.at[t], low_ref.at[t], 1)
+    w_own(5)
     w_pass(0, 0)
     w_start(1, 2)
     cq_in.wait()
@@ -936,30 +935,30 @@
     arrive(low_ref.at[other], tp_r.at[1])
     low_parts()
     sum_start(2)
+    w_pass(1, 0)
     sum_start(0)
-    w_pass(1, 0)
     sum_start(1)
     w_pass(1, 1)
     sum_start(3)
     sum_relay(2)
     sum_relay(0)
-    w_pass(0, 5)
     w_start(0, 0)
     w_pass(2, 1)
+    w_pass(0, 5)
     sum_relay(3)
+    w_in[1][2].relay()
     sum_relay(1)
-    w_in[1][2].relay()
     sum_finish(2)
+    w_pass(2, 0)
+    sum_finish(0)
+    w_pass(1, 5)
+    w_start(1, 0)
     w_in[0][1].relay()
-    w_pass(1, 5)
-    sum_finish(0)
-    w_start(1, 0)
-    gram()
-    w_pass(2, 0)
     sum_finish(3)
     w_in[0][0].relay()
     w_start(2, 1)
     sum_finish(1)
+    gram()
     w_start(1, 1)
     loaded(m1_ref, 5)
     loaded(m2_ref, 6)
@@ -968,26 +967,26 @@
     w_pass(0, 4)
     w_pass(2, 5)
     w_pass(2, 2)
+    w_pass(1, 3)
     w_in[1][0].relay()
-    w_pass(1, 3)
     w_start(2, 0)
     ratio_in[0].relay()
+    ratio_start(1)
     w_pass(0, 3)
     ratio_start(3)
-    ratio_start(1)
     ratio_start(2)
     w_in[2][1].relay()
     w_start(2, 2)
     w_pass(2, 4)
-    w_pass(1, 4)
     w_pass(2, 3)
     ratio_in[1].relay()
     ratio_in[2].relay()
     ratio_in[3].relay()
+    w_pass(1, 4)
     w_in[0][2].relay()
     w_in[2][2].relay()
+    w_in[1][1].relay()
     w_in[2][0].relay()
-    w_in[1][1].relay()
     arrive(ratio_ref.at[at(corner * own, own, own)], ac_r.at[0])
     qs = squares(0, slice(0, qc)) / (width * qc * 2)
     vs = squares(1, slice(qc, cols)) / (width * (cols - qc) * 2)
@@ -1063,15 +1062,15 @@
             dma((7,)),
             dma((3,)),
             dma((4,)),
-            dma((3, 3)),
-            dma((4, m)),
-            dma((3, n, 2)),
+            dma((3, 2)),
+            dma((3, m)),
+            dma((3, n)),
             dma((3,)),
-            dma((4, 2)),
-            dma((4, 2)),
             dma((4,)),
             dma((4,)),
-            dma((4, 2)),
+            dma((4,)),
+            dma((4,)),
+            dma((4,)),
             dma((1,)),
             dma((3,)),
             dma((3,)),

time: 68 us -> 67.1 us (0.987)
  Pallas kernels: 67.1 us -> 66.3 us
    pallas_call x1, Pallas kernels: 62.3 us -> 61.4 us  [run_line_exchange(): pl.pallas_call(functools.partial(line_exchange, quarter, chunks, rests),...]
where the time goes in v5:
time: 67.1 us; the launch traced here: 66.9 us
  Pallas kernels  66.3 us (99%)
    pallas_call x1, Pallas kernels, run_line_exchange(): pl.pallas_call(functools.partial(line_exchange, quarter, chunks, rests),...  61.4 us
    pallas_call x1, Pallas kernels, run_line_finish(): pl.pallas_call(functools.partial(line_finish, 8), in_specs=[vmem] * 8, ou...  4.86 us

profile of v5, /device:TPU:0, one launch (start us, length us, event | category | flops | bytes accessed | tf_op | source)
XLA Modules:
  0.0 66.9 jit_solution(12229204242805002053)
XLA Ops:
  0.6 61.4 %shard_map.186 = (bf16[2048,1536]{1,0:T(8,128)(2,1)S(1)}, bf16[2,2048,256]{2,1,0:T(8,128)(2,1)S(1)}, bf16[256,1536]{1,0:T(8,128)(2,1)S(1)}, f32[512,1536]{1,0:T(...) custom-call(bf16[768,2048]{1,0:T(8,128)(2,1)} %x_hbm.1, ...), custom_call_target="tpu_custom_call" | custom-call | tf_op jit(solution)/shard_map/pallas_call | solution.py:1030
  62.1 4.9 %shard_map.187 = (f32[512,512]{1,0:T(8,128)}, f32[512,1024]{1,0:T(8,128)}, f32[512,512]{1,0:T(8,128)}, f32[512,1024]{1,0:T(8,128)}, f32[64,512]{1,0:T(8,128)}, /...) custom-call(bf16[2048,1536]{1,0:T(8,128)(2,1)S(1)} %get-tuple-elemen, ...), custom_call_target="tpu_custom_call" | custom-call | tf_op jit(solution)/shard_map/pallas_call | solution.py:1149

commit v6 on v5

--- a/solution.py
+++ b/solution.py
@@ -1118,7 +1118,7 @@
         (m2_ref, right, v2_out),
     )
     copies = [
-        pltpu.make_async_copy(src.at[:, cut], dst, sem.at[n])
+        pltpu.make_async_copy(src.at[:, cut], dst, sem.at[n // 2])
         for n, (src, cut, dst) in enumerate(outs)
     ]
     for c in copies:
@@ -1132,12 +1132,10 @@
             raw = jnp.dot(f_ref[n, span], ratio_ref[:, cut], preferred_element_type=F32)
             raw = raw * scale_ref[n : n + 1, 0:1]
             c_ref[span, cut] = (w_ref[span, cut].astype(F32) - RATE * raw).astype(BF)
-            pltpu.make_async_copy(c_ref.at[span, cut], dst.at[span], sem.at[8 + n]).start()
-
-    for c in copies:
-        c.wait()
-    for n, cut, dst in ((0, left, qcopy_out), (1, right, vcopy_out)):
-        pltpu.make_async_copy(c_ref.at[:, cut], dst, sem.at[8 + n]).wait()
+            pltpu.make_async_copy(c_ref.at[span, cut], dst.at[span], sem.at[4]).start()
+
+    for n, ref in enumerate((d_ref, m_ref, m1_ref, m2_ref, c_ref)):
+        pltpu.make_async_copy(ref, ref, sem.at[n]).wait()
 
 
 def run_line_finish(weights, factors, ratio, masters, m1, m2, scale, directions, qc):
@@ -1162,7 +1160,7 @@
             shape((width, qc), BF),
             shape((width, vc), BF),
         ],
-        scratch_shapes=[pltpu.VMEM((width, cols), BF), pltpu.SemaphoreType.DMA((10,))],
+        scratch_shapes=[pltpu.VMEM((width, cols), BF), pltpu.SemaphoreType.DMA((5,))],
         compiler_params=pltpu.CompilerParams(vmem_limit_bytes=16 * 1024 * 1024),
     )(weights, factors, ratio, masters, m1, m2, scale, directions)
 

time: 67.1 us -> 67.1 us (level)
  no operation moved by 1% of the time
where the time goes in v6:
time: 67.1 us; the launch traced here: 66.9 us
  Pallas kernels  66.2 us (99%)
    pallas_call x1, Pallas kernels, run_line_exchange(): pl.pallas_call(functools.partial(line_exchange, quarter, chunks, rests),...  61.4 us
    pallas_call x1, Pallas kernels, run_line_finish(): pl.pallas_call(functools.partial(line_finish, 8), in_specs=[vmem] * 8, ou...  4.82 us

profile of v6, /device:TPU:0, one launch (start us, length us, event | category | flops | bytes accessed | tf_op | source)
XLA Modules:
  0.0 66.9 jit_solution(14499864442350381555)
XLA Ops:
  0.6 61.4 %shard_map.186 = (bf16[2048,1536]{1,0:T(8,128)(2,1)S(1)}, bf16[2,2048,256]{2,1,0:T(8,128)(2,1)S(1)}, bf16[256,1536]{1,0:T(8,128)(2,1)S(1)}, f32[512,1536]{1,0:T(...) custom-call(bf16[768,2048]{1,0:T(8,128)(2,1)} %x_hbm.1, ...), custom_call_target="tpu_custom_call" | custom-call | tf_op jit(solution)/shard_map/pallas_call | solution.py:1030
  62.1 4.8 %shard_map.187 = (f32[512,512]{1,0:T(8,128)}, f32[512,1024]{1,0:T(8,128)}, f32[512,512]{1,0:T(8,128)}, f32[512,1024]{1,0:T(8,128)}, f32[64,512]{1,0:T(8,128)}, /...) custom-call(bf16[2048,1536]{1,0:T(8,128)(2,1)S(1)} %get-tuple-elemen, ...), custom_call_target="tpu_custom_call" | custom-call | tf_op jit(solution)/shard_map/pallas_call | solution.py:1147
